TPU v7x, 32 devices: a whole 2x2x4 slice. The times are simulated.
32 devices in a mesh: sp: 8 (over z, x), dp: 4 (over y, core).
Axes of the slice: x: 2, y: 2, z: 4, core: 2. Of those that a mesh axis runs over, the one named last changes fastest.
Arguments:
- residual_in: bfloat16 [4, 1024, 2048], P('dp', 'sp'), may hold values from -6 to 6
- ssm_input: bfloat16 [4, 1024, 2048], P('dp', 'sp'), may hold values from -6 to 6
- state_b: bfloat16 [4, 1024, 2048], P('dp', 'sp'), may hold values from -6 to 6
- state_c: bfloat16 [4, 1024, 2048], P('dp', 'sp'), may hold values from -6 to 6
- step_raw: bfloat16 [4, 1024, 64], P('dp', 'sp'), may hold values from -4 to 3
- gate_input: bfloat16 [4, 1024, 2048], P('dp', 'sp'), may hold values from -6 to 6
- conv_x: float32 [7, 2048], P(None, 'sp'), may hold values from -2 to 2
- conv_b: float32 [7, 2048], P(None, 'sp'), may hold values from -2 to 2
- conv_c: float32 [7, 2048], P(None, 'sp'), may hold values from -2 to 2
- decay_rate: float32 [2, 32], P(None, 'sp'), may hold values from 0 to 1, as said below
- mix_gain: float32 [2048], replicated, may hold values from 0.1 to 1.9
- out_weight: bfloat16 [2048, 2048], P('dp'), may hold values from -0.125 to 0.125
- ffn_gain: float32 [2048], replicated, may hold values from 0.1 to 1.9
- routing: int32 [4, 1024, 4], P('dp', 'sp'), may hold values from 0 to 31, all different within a row; in each aligned block of 128 rows (0 to 127, 128 to 255, ..., all dimensions but the last counted through in order) at most 32 rows name the same one
- route_weight: float32 [4, 1024, 4], P('dp', 'sp'), may hold values from 0.1 to 0.6
- gate_w: bfloat16 [32, 2048, 1024], P(('sp', 'dp')), may hold values from -60 to 60
- up_w: bfloat16 [32, 2048, 1024], P(('sp', 'dp')), may hold values from -60 to 60
- down_w: bfloat16 [32, 1024, 2048], P(('sp', 'dp')), may hold values from -0.1875 to 0.1875
Outputs:
- block_out: bfloat16 [4, 1024, 2048], P('dp', 'sp')
Inputs may be any that keep to these rules, and one draw needn't show every extreme that they name: `routing`: each row names 4 different experts; within the rows of one device no expert is named by more than 32 rows, a bound that some block reaches. `decay_rate`: Positive.
All inputs are finite; a program needn't handle non-finite values.
Results may differ from a plain program's by a relative error of at most 0.0082.
Values may be sent and summed in bfloat16 or wider, within the bound.
No kernel may reach another device: no remote copies, remote signals or barrier semaphores. Data moves between devices by JAX's collectives and lax.ppermute only.
A program may use at most 128 MiB of HBM per device.

v0:
```python
import jax
import jax.numpy as jnp
from jax import lax
from jax.sharding import PartitionSpec as P

HEAD_DIM = 64
STATE = 128
BLOCK = 128
NORM_GROUPS = 4


highest = lax.Precision.HIGHEST
epsilon = 1e-05
clamp_limit = 7.0
sigmoid_slope = 1.702


def centred_conv(values, taps):
    half_width = taps.shape[0] // 2
    padded = jnp.pad(values, ((half_width, half_width), (0, 0)))
    total = jnp.zeros_like(values)
    for offset in range(taps.shape[0]):
        total = total + padded[offset : offset + values.shape[0]] * taps[offset]
    return total


def ssd_direction(signal, step_size, rates, write_map, read_map):
    length = signal.shape[0]
    head_count = signal.shape[1]
    head_width = signal.shape[2]
    group_count = write_map.shape[1]
    state_width = write_map.shape[2]
    per_group = head_count // group_count
    blocks = length // BLOCK
    scaled = (signal * step_size[..., None]).reshape(
        blocks, BLOCK, group_count, per_group, head_width
    )
    cumulative = jnp.cumsum(
        (-step_size * rates).reshape(blocks, BLOCK, group_count, per_group), axis=1
    )
    write_block = write_map.reshape(blocks, BLOCK, group_count, state_width)
    read_block = read_map.reshape(blocks, BLOCK, group_count, state_width)
    spread = cumulative[:, :, None] - cumulative[:, None]
    lower_mask = (lax.iota(jnp.int32, BLOCK)[:, None] >= lax.iota(jnp.int32, BLOCK)[None, :])[
        None, :, :, None, None
    ]
    weight_in = jnp.exp(jnp.where(lower_mask, spread, -jnp.inf))
    intersect = jnp.einsum("clgn,csgn->clsg", read_block, write_block, precision=highest)
    inside = jnp.einsum(
        "clsgk,csgkp->clgkp", intersect[..., None] * weight_in, scaled, precision=highest
    )
    to_end = jnp.exp(cumulative[:, -1:] - cumulative)
    states = jnp.einsum(
        "csgn,csgkp->cgkpn", write_block, scaled * to_end[..., None], precision=highest
    )
    carry_decay = jnp.exp(cumulative[:, -1])

    def advance(running, block_pair):
        block_state, factor = block_pair
        return (factor[..., None, None] * running + block_state, running)

    initial = jnp.zeros((group_count, per_group, head_width, state_width), jnp.float32)
    _, entering = lax.scan(advance, initial, (states, carry_decay))
    carried = (
        jnp.einsum("clgn,cgkpn->clgkp", read_block, entering, precision=highest)
        * jnp.exp(cumulative)[..., None]
    )
    return (inside + carried).reshape(length, head_count, head_width)


def both_ways(signal, steps_fwd, steps_bwd, rates, write_map, read_map):
    forward = ssd_direction(signal, steps_fwd, rates[0], write_map, read_map)
    backward = ssd_direction(
        jnp.flip(signal, 0),
        jnp.flip(steps_bwd, 0),
        rates[1],
        jnp.flip(write_map, 0),
        jnp.flip(read_map, 0),
    )
    return forward + jnp.flip(backward, 0)


def scale_rows(values, gains):
    return values * lax.rsqrt(jnp.mean(values * values, axis=-1, keepdims=True) + epsilon) * gains


def group_scale(values, gains):
    shaped = values.reshape(values.shape[:-1] + (NORM_GROUPS, values.shape[-1] // NORM_GROUPS))
    shaped = shaped * lax.rsqrt(jnp.mean(shaped * shaped, axis=-1, keepdims=True) + epsilon)
    return shaped.reshape(values.shape) * gains


def expert_apply(rows, gate_mat, up_mat, down_mat):
    gate_value = jnp.minimum(
        jnp.dot(rows, gate_mat, preferred_element_type=jnp.float32), clamp_limit
    )
    up_value = jnp.clip(
        jnp.dot(rows, up_mat, preferred_element_type=jnp.float32), -clamp_limit, clamp_limit
    )
    active = ((up_value + 1.0) * gate_value * jax.nn.sigmoid(sigmoid_slope * gate_value)).astype(
        jnp.bfloat16
    )
    return jnp.dot(active, down_mat, preferred_element_type=jnp.float32).astype(jnp.bfloat16)


def per_device(
    residual_in,
    ssm_input,
    state_b,
    state_c,
    step_raw,
    gate_input,
    conv_x,
    conv_b,
    conv_c,
    decay_rate,
    mix_gain,
    out_weight,
    ffn_gain,
    routing,
    route_weight,
    gate_w,
    up_w,
    down_w,
):
    signal_loc, write_loc, read_loc, step_loc = (
        lax.all_to_all(ssm_input, "sp", split_axis=2, concat_axis=1, tiled=True),
        lax.all_to_all(state_b, "sp", split_axis=2, concat_axis=1, tiled=True),
        lax.all_to_all(state_c, "sp", split_axis=2, concat_axis=1, tiled=True),
        lax.all_to_all(step_raw, "sp", split_axis=2, concat_axis=1, tiled=True),
    )
    length = signal_loc.shape[1]
    head_local = decay_rate.shape[1]
    signal = jax.nn.silu(centred_conv(signal_loc[0].astype(jnp.float32), conv_x)).reshape(
        length, head_local, HEAD_DIM
    )
    write_map = jax.nn.silu(centred_conv(write_loc[0].astype(jnp.float32), conv_b)).reshape(
        length, -1, STATE
    )
    read_map = jax.nn.silu(centred_conv(read_loc[0].astype(jnp.float32), conv_c)).reshape(
        length, -1, STATE
    )
    step_pair = jax.nn.softplus(step_loc[0].astype(jnp.float32).reshape(length, head_local, 2))
    mixed_heads = both_ways(
        signal, step_pair[..., 0], step_pair[..., 1], decay_rate, write_map, read_map
    )
    mixed_heads = mixed_heads.reshape(1, length, head_local * HEAD_DIM).astype(jnp.bfloat16)
    mixed_tokens = lax.all_to_all(mixed_heads, "sp", split_axis=1, concat_axis=2, tiled=True)
    token_count = residual_in.shape[1]
    model_width = residual_in.shape[2]
    gated = mixed_tokens[0].astype(jnp.float32) * jax.nn.silu(gate_input[0].astype(jnp.float32))
    mixed = group_scale(gated, mix_gain).astype(jnp.bfloat16)
    projected = jnp.dot(
        mixed,
        lax.all_gather(out_weight, "dp", axis=0, tiled=True),
        preferred_element_type=jnp.float32,
    )
    stream = residual_in[0].astype(jnp.float32) + projected
    ffn_input = scale_rows(stream, ffn_gain).astype(jnp.bfloat16)
    sp_count = lax.axis_size("sp")
    dp_count = lax.axis_size("dp")
    experts_all = sp_count * dp_count
    top_count = routing.shape[2]
    assigned = token_count * top_count
    capacity = 2 * assigned // experts_all
    flat_expert = routing.reshape(assigned)
    one_hot = (flat_expert[:, None] == lax.iota(jnp.int32, experts_all)[None, :]).astype(
        jnp.bfloat16
    )
    earlier = (
        lax.iota(jnp.int32, assigned)[:, None] > lax.iota(jnp.int32, assigned)[None, :]
    ).astype(jnp.bfloat16)
    before = jnp.dot(earlier, one_hot, preferred_element_type=jnp.float32)
    slot_index = jnp.sum(before * one_hot.astype(jnp.float32), axis=1).astype(jnp.int32)
    target = flat_expert * capacity + slot_index
    source_token = (
        jnp.zeros((experts_all * capacity,), jnp.int32)
        .at[target]
        .set(lax.iota(jnp.int32, assigned) // top_count)
    )
    filled = jnp.zeros((experts_all * capacity,), jnp.bool_).at[target].set(True)
    outgoing = jnp.where(filled[:, None], ffn_input[source_token], jnp.zeros((), jnp.bfloat16))
    arrived = lax.all_to_all(
        outgoing.reshape(experts_all, 1, capacity, model_width),
        ("sp", "dp"),
        split_axis=0,
        concat_axis=1,
        tiled=True,
    )
    served = expert_apply(arrived.reshape(-1, model_width), gate_w[0], up_w[0], down_w[0]).reshape(
        arrived.shape
    )
    returned = lax.all_to_all(served, ("sp", "dp"), split_axis=1, concat_axis=0, tiled=True)
    answers = returned.reshape(experts_all * capacity, model_width)[target].reshape(
        token_count, top_count, model_width
    )
    routed = jnp.sum(answers.astype(jnp.float32) * route_weight[0][:, :, None], axis=1)
    return (stream + routed).astype(jnp.bfloat16)[None]


def solution(mesh):
    return jax.shard_map(
        per_device,
        mesh=mesh,
        in_specs=(
            P("dp", "sp", None),
            P("dp", "sp", None),
            P("dp", "sp", None),
            P("dp", "sp", None),
            P("dp", "sp", None),
            P("dp", "sp", None),
            P(None, "sp"),
            P(None, "sp"),
            P(None, "sp"),
            P(None, "sp"),
            P(),
            P("dp", None),
            P(),
            P("dp", "sp", None),
            P("dp", "sp", None),
            P(("sp", "dp"), None, None),
            P(("sp", "dp"), None, None),
            P(("sp", "dp"), None, None),
        ),
        out_specs=P("dp", "sp", None),
        check_vma=False,
    )
```

profile of v0, /device:TPU:0, one launch (start us, length us, event | category | flops | bytes accessed | tf_op | source)
XLA Modules:
  0.0 593.2 jit_solution(14544832548649737198)
XLA Ops:
  9.2 7.3 %all-to-all-start.1 = ((bf16[8,2,512]{2,1,0:T(2,128)(2,1)}), bf16[8,2,512]{2,1,0:T(2,128)(2,1)S(1)}, u32[]{:S(2)}, u32[]{:S(2)}) async-start(bf16[8,2,512]{2,1,0:T(2,128)(2,1)} %reshape.329), calls=%async_computation.1 | async-start | bytes 32768 | tf_op jit(solution)/shard_map/all_to_all | solution.py:130
  25.2 11.5 %reduce.8 = bf16[2048,128]{1,0:T(8,128)(2,1)S(1)} reduce(bf16[2048,1,128]{2,1,0:T(2,128)(2,1)S(1)} %bitcast.256, bf16[]{:T(256)} %broadcast.189), dimensions={1}, to_apply=%bitcast.193.reduce_sub_computation | reduce | bytes 1048578
  38.4 11.5 %reduce.7 = bf16[2048,128]{1,0:T(8,128)(2,1)S(1)} reduce(bf16[2048,1,128]{2,1,0:T(2,128)(2,1)S(1)} %bitcast.257, bf16[]{:T(256)} %broadcast.189), dimensions={1}, to_apply=%bitcast.191.reduce_sub_computation | reduce | bytes 1048578
  51.6 11.8 %reduce.9 = bf16[2048,128]{1,0:T(8,128)(2,1)S(1)} reduce(bf16[2048,1,128]{2,1,0:T(2,128)(2,1)S(1)} %bitcast.258, bf16[]{:T(256)} %broadcast.189), dimensions={1}, to_apply=%bitcast.195.reduce_sub_computation | reduce | bytes 1048578
  64.4 6.0 %all-to-all-start = ((bf16[8,2,16384]{2,1,0:T(2,128)(2,1)}), bf16[8,2,16384]{2,1,0:T(2,128)(2,1)}, u32[]{:S(2)}, u32[]{:S(2)}) async-start(bf16[8,2,16384]{2,1,0:T(2,128)(2,1)} %reshape.333), calls=%async_computation | async-start | bytes 1048576 | tf_op jit(solution)/shard_map/all_to_all | solution.py:127
  71.8 47.4 %fusion.95 = f32[8,128,2,2]{3,0,1,2:T(8,128)S(1)} fusion(f32[8,128,2,2]{3,0,1,2:T(8,128)S(1)} %copy.202), kind=kOutput, calls=%fused_computation.155 | output fusion | flops 520192 | bytes 32768 | tf_op jit(solution)/shard_map/jit(cumsum)/reduce_window_sum | solution.py:38
  120.0 47.4 %fusion.94 = f32[8,128,2,2]{3,0,1,2:T(8,128)S(1)} fusion(f32[8,128,2,2]{3,0,1,2:T(8,128)S(1)} %copy.183), kind=kOutput, calls=%fused_computation.154 | output fusion | flops 520192 | bytes 32768 | tf_op jit(solution)/shard_map/jit(cumsum)/reduce_window_sum | solution.py:38
  170.5 6.0 %all-to-all-start.2 = ((bf16[8,2,16384]{2,1,0:T(2,128)(2,1)}), bf16[8,2,16384]{2,1,0:T(2,128)(2,1)}, u32[]{:S(2)}, u32[]{:S(2)}) async-start(bf16[8,2,16384]{2,1,0:T(2,128)(2,1)} %reshape.331), calls=%async_computation.2 | async-start | bytes 1048576 | tf_op jit(solution)/shard_map/all_to_all | solution.py:128
  190.0 6.2 %all-to-all-start.3 = ((bf16[8,2,16384]{2,1,0:T(2,128)(2,1)}), bf16[8,2,16384]{2,1,0:T(2,128)(2,1)}, u32[]{:S(2)}, u32[]{:S(2)}) async-start(bf16[8,2,16384]{2,1,0:T(2,128)(2,1)} %reshape.335), calls=%async_computation.3 | async-start | bytes 1048576 | tf_op jit(solution)/shard_map/all_to_all | solution.py:129
  203.0 6.8 %rev.20 = f32[1024,2,128]{2,0,1:T(8,128)S(1)} reverse(f32[1024,2,128]{2,0,1:T(8,128)} %copy_bitcast_fusion.1), dimensions={0} | reverse | bytes 2097152 | tf_op jit(solution)/shard_map/jit(_flip)/rev | solution.py:77
  218.3 6.2 %copy_bitcast_fusion = f32[1024,2,128]{2,0,1:T(8,128)} fusion(f32[256]{0:T(256)} %bitcast.284, f32[256]{0:T(256)} %bitcast.286, f32[256]{0:T(256)S(1)} %bitcast.276, f32[1024,256]{1,0:T(8,128)} %bitcast.240, f32[256]{0:T(256)S(1)} %bitcast.278, f32[256]{0:T(256)S(1)} %bitcast.280, f32[256]{0:T(256)} %bitcast.282, f32[256]{0:T(256)S(1)} %bitcast.274), kind=kLoop, calls=%fused_computation.43 | loop fusion | flops 4456448 | bytes 2104320 | tf_op jit(solution)/shard_map/reshape | solution.py:140
  224.5 6.8 %rev.21 = f32[1024,2,128]{2,0,1:T(8,128)S(1)} reverse(f32[1024,2,128]{2,0,1:T(8,128)} %copy_bitcast_fusion), dimensions={0} | reverse | bytes 2097152 | tf_op jit(solution)/shard_map/jit(_flip)/rev | solution.py:78
  241.9 18.6 %while.27 = (s32[]{:T(128)}, f32[2,2,64,128]{3,2,1,0:T(8,128)S(1)}, f32[8,2,2,64,128]{4,3,2,1,0:T(8,128)}, f32[8,2,2]{2,1,0:T(2,128)}, f32[8,2,2,64,128]{4,3,2,1,0:T(8,128)}, /*index=5*/s32[]{:T(128)}, s32[]{:T(128)}) while((s32[]{:T(128)}, f32[2,2,64,128]{3,2,1,0:T(8,128)S(1)}, f32[8,2,2,64,128]{4,3,2,1,0:T(8,128)}, ...), condition=%wide.region_5.6_spmd.clone, body=%wide.region_4.5_spmd.clone.sunk | while | flops 131075 | bytes 656016 | solution.py:63
  271.5 5.6 rev.22
  293.4 13.7 %while.26 = (s32[]{:T(128)}, f32[2,2,64,128]{3,2,1,0:T(8,128)S(1)}, f32[8,2,2,64,128]{4,3,2,1,0:T(8,128)S(1)}, f32[8,2,2]{2,1,0:T(2,128)}, f32[8,2,2,64,128]{4,3,2,1,0:T(8,128)}, /*index=5*/s32[]{:T(128)}, s32[]{:T(128)}) while((s32[]{:T(128)}, f32[2,2,64,128]{3,2,1,0:T(8,128)S(1)}, f32[8,2,2,64,128]{4,3,2,1,0:T(8,128)S(1)}, ...), condition=%wide.region_2.3_spmd.clone, body=%wide.region_1.2_spmd.clone.sunk | while | flops 131075 | bytes 655508 | solution.py:63
  309.4 5.6 fusion.24
  321.5 6.0 %all-to-all-start.4 = ((bf16[8,2,16384]{2,1,0:T(2,128)(2,1)}), bf16[8,2,16384]{2,1,0:T(2,128)(2,1)S(1)}, u32[]{:S(2)}, u32[]{:S(2)}) async-start(bf16[8,2,16384]{2,1,0:T(2,128)(2,1)} %reshape.337), calls=%async_computation.4 | async-start | bytes 1048576 | tf_op jit(solution)/shard_map/all_to_all | solution.py:148
  334.1 5.7 all-to-all-done.4
  348.9 6.0 %gather_fusion = bf16[1024,2048]{1,0:T(8,128)(2,1)} fusion(bf16[128,2048]{1,0:T(8,128)(2,1)S(1)} %multiply_convert_fusion.1, s32[1024]{0:T(1024)S(1)} %fusion.78), kind=kCustom, calls=%fused_computation | custom fusion | bytes 8392704 | tf_op jit(solution)/shard_map/gather | solution.py:182
  357.5 97.6 %all_to_all.28 = bf16[32,1,32,2048]{3,2,1,0:T(8,128)(2,1)S(1)} all-to-all(bf16[32,1,32,2048]{3,2,1,0:T(8,128)(2,1)S(1)} %broadcast_select_fusion), channel_id=1, replica_groups=mesh['sp'=8,'dp'=4] {'sp','dp'}, dimensions={0} | all-to-all | bytes 8388608 | tf_op jit(solution)/shard_map/all_to_all | solution.py:183
  459.7 5.7 multiply_convert_fusion
  465.3 6.1 %fusion.6 = bf16[1024,2048]{1,0:T(8,128)(2,1)} fusion(bf16[1024,1024]{1,0:T(8,128)(2,1)S(1)} %multiply_convert_fusion, bf16[1,1024,2048]{2,1,0:T(8,128)(2,1)S(1)} %copy-done.35), kind=kOutput, calls=%fused_computation.19 | convolution fusion | flops 4297064448 | bytes 10485760 | tf_op jit(solution)/shard_map/dot_general | solution.py:103
  475.6 94.1 %all-to-all-done.6 = bf16[1,32,32,2048]{3,2,0,1:T(8,128)(2,1)} async-done(((bf16[1,32,32,2048]{3,2,0,1:T(8,128)(2,1)}), bf16[1,32,32,2048]{3,2,0,1:T(8,128)(2,1)}, u32[]{:S(2)}, u32[]{:S(2)}) %all-to-all-start.6) | async-done | bytes 4194336 | tf_op jit(solution)/shard_map/all_to_all | solution.py:193
  569.7 7.1 %gather_fusion.1 = bf16[512,2048]{1,0:T(8,128)(2,1)S(1)} fusion(bf16[1024,2048]{1,0:T(8,128)(2,1)} %bitcast.69, s32[1024]{0:T(1024)S(1)} %pad_clamp_fusion), kind=kCustom, calls=%fused_computation.1 | custom fusion | bytes 4196352 | tf_op jit(solution)/shard_map/gather | solution.py:194
  (254 shorter events, 163.4 us)
Async XLA Ops:
  6.5 31.1 %copy-start.7 = (bf16[1,128,2048]{2,1,0:T(8,128)(2,1)S(1)}, bf16[1,128,2048]{2,1,0:T(8,128)(2,1)}, u32[]{:S(2)}) copy-start(bf16[1,128,2048]{2,1,0:T(8,128)(2,1)} %param.24) | copy-start | bytes 1572868
  9.2 55.2 %all-to-all-start.1 = ((bf16[8,2,512]{2,1,0:T(2,128)(2,1)}), bf16[8,2,512]{2,1,0:T(2,128)(2,1)S(1)}, u32[]{:S(2)}, u32[]{:S(2)}) async-start(bf16[8,2,512]{2,1,0:T(2,128)(2,1)} %reshape.329), calls=%async_computation.1 | async-start | bytes 32768 | tf_op jit(solution)/shard_map/all_to_all | solution.py:130
  16.5 327.5 %all-gather.2.cloned.1.call-start = ((), (), s32[]{:S(2)}) async-start(), calls=%async_computation.7 | async-start | bytes 10485760 | tf_op jit(solution)/shard_map/all_gather | solution.py:155
  22.7 28.1 %copy-start.8 = (bf16[1,128,2048]{2,1,0:T(8,128)(2,1)S(1)}, bf16[1,128,2048]{2,1,0:T(8,128)(2,1)}, u32[]{:S(2)}) copy-start(bf16[1,128,2048]{2,1,0:T(8,128)(2,1)} %param.25) | copy-start | bytes 1572868
  64.4 106.2 %all-to-all-start = ((bf16[8,2,16384]{2,1,0:T(2,128)(2,1)}), bf16[8,2,16384]{2,1,0:T(2,128)(2,1)}, u32[]{:S(2)}, u32[]{:S(2)}) async-start(bf16[8,2,16384]{2,1,0:T(2,128)(2,1)} %reshape.333), calls=%async_computation | async-start | bytes 1048576 | tf_op jit(solution)/shard_map/all_to_all | solution.py:127
  170.5 19.5 %all-to-all-start.2 = ((bf16[8,2,16384]{2,1,0:T(2,128)(2,1)}), bf16[8,2,16384]{2,1,0:T(2,128)(2,1)}, u32[]{:S(2)}, u32[]{:S(2)}) async-start(bf16[8,2,16384]{2,1,0:T(2,128)(2,1)} %reshape.331), calls=%async_computation.2 | async-start | bytes 1048576 | tf_op jit(solution)/shard_map/all_to_all | solution.py:128
  190.0 19.9 %all-to-all-start.3 = ((bf16[8,2,16384]{2,1,0:T(2,128)(2,1)}), bf16[8,2,16384]{2,1,0:T(2,128)(2,1)}, u32[]{:S(2)}, u32[]{:S(2)}) async-start(bf16[8,2,16384]{2,1,0:T(2,128)(2,1)} %reshape.335), calls=%async_computation.3 | async-start | bytes 1048576 | tf_op jit(solution)/shard_map/all_to_all | solution.py:129
  200.2 15.5 %copy-start = (f32[1,8,128,256]{3,2,1,0:T(8,128)}, f32[1,8,128,256]{3,2,1,0:T(8,128)S(1)}, u32[]{:S(2)}) copy-start(f32[1,8,128,256]{3,2,1,0:T(8,128)S(1)} %copy.175) | copy-start | bytes 3145732
  203.0 15.3 %copy-start.10 = (f32[1,256]{1,0:T(1,128)S(1)}, f32[1,256]{1,0:T(1,128)}, u32[]{:S(2)}) copy-start(f32[1,256]{1,0:T(1,128)} %get-tuple-element.177) | copy-start | bytes 3076
  203.0 15.3 %copy-start.11 = (f32[1,256]{1,0:T(1,128)S(1)}, f32[1,256]{1,0:T(1,128)}, u32[]{:S(2)}) copy-start(f32[1,256]{1,0:T(1,128)} %get-tuple-element.178) | copy-start | bytes 3076
  203.0 15.3 %copy-start.12 = (f32[1,256]{1,0:T(1,128)S(1)}, f32[1,256]{1,0:T(1,128)}, u32[]{:S(2)}) copy-start(f32[1,256]{1,0:T(1,128)} %get-tuple-element.179) | copy-start | bytes 3076
  203.0 15.3 %copy-start.13 = (f32[1,256]{1,0:T(1,128)S(1)}, f32[1,256]{1,0:T(1,128)}, u32[]{:S(2)}) copy-start(f32[1,256]{1,0:T(1,128)} %get-tuple-element.180) | copy-start | bytes 3076
  240.8 23.3 %copy-start.3 = (f32[32,8,8,128]{3,2,1,0:T(8,128)S(1)}, f32[32,8,8,128]{3,2,1,0:T(8,128)}, u32[]{:S(2)}) copy-start(f32[32,8,8,128]{3,2,1,0:T(8,128)} %copy.245) | copy-start | bytes 3145732
  269.6 8.7 %copy-start.1 = (f32[1,8,128,256]{3,2,1,0:T(8,128)S(1)}, f32[1,8,128,256]{3,2,1,0:T(8,128)}, u32[]{:S(2)}) copy-start(f32[1,8,128,256]{3,2,1,0:T(8,128)} %copy-done) | copy-start | bytes 3145732
  269.6 8.7 %copy-start.19 = (f32[1,256]{1,0:T(1,128)S(1)}, f32[1,256]{1,0:T(1,128)}, u32[]{:S(2)}) copy-start(f32[1,256]{1,0:T(1,128)} %get-tuple-element.191) | copy-start | bytes 3076
  269.6 8.7 %copy-start.21 = (f32[1,256]{1,0:T(1,128)S(1)}, f32[1,256]{1,0:T(1,128)}, u32[]{:S(2)}) copy-start(f32[1,256]{1,0:T(1,128)} %get-tuple-element.192) | copy-start | bytes 3076
  269.6 8.7 %copy-start.23 = (f32[1,256]{1,0:T(1,128)S(1)}, f32[1,256]{1,0:T(1,128)}, u32[]{:S(2)}) copy-start(f32[1,256]{1,0:T(1,128)} %get-tuple-element.193) | copy-start | bytes 3076
  293.3 16.1 %copy-start.6 = (f32[8,128,2,2,64]{1,0,4,3,2:T(8,128)S(1)}, f32[8,128,2,2,64]{1,0,4,3,2:T(8,128)}, u32[]{:S(2)}) copy-start(f32[8,128,2,2,64]{1,0,4,3,2:T(8,128)} %get-tuple-element.170) | copy-start | bytes 3145732
  315.9 11.6 %copy-start.9 = (bf16[1,128,2048]{2,1,0:T(8,128)(2,1)S(1)}, bf16[1,128,2048]{2,1,0:T(8,128)(2,1)}, u32[]{:S(2)}) copy-start(bf16[1,128,2048]{2,1,0:T(8,128)(2,1)} %param.27) | copy-start | bytes 1572868
  315.9 12.1 %copy-start.31 = (s32[1,128,4]{1,2,0:T(4,128)S(1)}, s32[1,128,4]{1,2,0:T(4,128)}, u32[]{:S(2)}) copy-start(s32[1,128,4]{1,2,0:T(4,128)} %param.35) | copy-start | bytes 6148
  321.5 18.2 %all-to-all-start.4 = ((bf16[8,2,16384]{2,1,0:T(2,128)(2,1)}), bf16[8,2,16384]{2,1,0:T(2,128)(2,1)S(1)}, u32[]{:S(2)}, u32[]{:S(2)}) async-start(bf16[8,2,16384]{2,1,0:T(2,128)(2,1)} %reshape.337), calls=%async_computation.4 | async-start | bytes 1048576 | tf_op jit(solution)/shard_map/all_to_all | solution.py:148
  328.3 15.3 %copy-start.29 = (f32[2048]{0:T(1024)S(1)}, f32[2048]{0:T(1024)}, u32[]{:S(2)}) copy-start(f32[2048]{0:T(1024)} %param.32) | copy-start | bytes 24580
  357.5 97.6 %copy-start.33 = (bf16[1,2048,1024]{2,1,0:T(8,128)(2,1)S(1)}, bf16[1,2048,1024]{2,1,0:T(8,128)(2,1)}, u32[]{:S(2)}) copy-start(bf16[1,2048,1024]{2,1,0:T(8,128)(2,1)} %param.37) | copy-start | bytes 12582916
  471.5 98.2 %all-to-all-start.6 = ((bf16[1,32,32,2048]{3,2,0,1:T(8,128)(2,1)}), bf16[1,32,32,2048]{3,2,0,1:T(8,128)(2,1)}, u32[]{:S(2)}, u32[]{:S(2)}) async-start(bf16[1,32,32,2048]{3,2,0,1:T(8,128)(2,1)} %bitcast.249), calls=%async_computation.6 | async-start | bytes 8388608 | tf_op jit(solution)/shard_map/all_to_all | solution.py:193
  (19 other events, 126.1 us)
Sparse Core Ops, SparseCore 0:
  18.9 59.6 all-gather.1
where the time goes:
time: 604 us; the launch traced here: 593 us
  other arithmetic  188 us (31%)
  local copies, waits for them, and re-layouts  107 us (18%)
  waiting for transfers between devices  101 us (17%)
  blocking collectives  97.6 us (16%)
  matrix products  49.4 us (8%)
  starting transfers between devices  35.4 us (6%)
  between operations  14.5 us (2%)
    all_to_all x1, blocking collectives, per_device(): lax.all_to_all(outgoing.reshape(experts_all, 1, capacity, model_width), (...  97.6 us
    another operation x2, other arithmetic, ssd_direction(): jnp.cumsum((-step_size * rates).reshape(blocks, BLOCK, group_count, per_g...  94.9 us
    all_to_all x1, waiting for transfers between devices, per_device(): lax.all_to_all(served, ('sp', 'dp'), split_axis=1, concat_axis=0, tiled=T...  94.1 us
    unnamed x8, other arithmetic  39.5 us
    unnamed x95, local copies, waits for them, and re-layouts  22.3 us
    add x16, other arithmetic, advance(): return (factor[..., None, None] * running + block_state, running)  15.7 us
  transfers between devices with their start and end apart: 7, of which 3 were waited for; matrix products, arithmetic and copies ran while one was open for 50% of the time, Pallas kernels for 0%

commit v1 on v0

v1 whole, which is shorter than its diff:
```python
import jax
import jax.numpy as jnp
from jax import lax
from jax.experimental import pallas as pl
from jax.experimental.pallas import tpu as pltpu
from jax.sharding import PartitionSpec as P

HEAD_DIM = 64
STATE = 128
NORM_GROUPS = 4
STEP_ROWS = 16

highest = lax.Precision.HIGHEST
epsilon = 1e-05
clamp_limit = 7.0
sigmoid_slope = 1.702
f32 = jnp.float32
bf16 = jnp.bfloat16


def pack_body(x_ref, b_ref, c_ref, s_ref, o_ref):
    tokens = x_ref.shape[0]
    o_ref[0, :tokens] = x_ref[...]
    o_ref[0, tokens : 2 * tokens] = b_ref[...]
    o_ref[0, 2 * tokens : 3 * tokens] = c_ref[...]
    o_ref[0, 3 * tokens :] = jnp.zeros((STEP_ROWS, o_ref.shape[2]), bf16)
    o_ref[0, 3 * tokens :, :tokens] = s_ref[0]


def pack_inputs(x, b, c, steps, parts):
    tokens, width = x.shape
    part_width = width // parts
    column = pl.BlockSpec((tokens, part_width), lambda i: (0, i))
    rows = 3 * tokens + STEP_ROWS
    return pl.pallas_call(
        pack_body,
        grid=(parts,),
        in_specs=[column, column, column, pl.BlockSpec((1, STEP_ROWS, tokens), lambda i: (i, 0, 0))],
        out_specs=pl.BlockSpec((1, rows, part_width), lambda i: (i, 0, 0)),
        out_shape=jax.ShapeDtypeStruct((parts, rows, part_width), bf16),
        name="pack_inputs",
    )(x, b, c, steps)


def nt_dot(left, right):
    return lax.dot_general(left, right, (((1,), (1,)), ((), ())), preferred_element_type=f32)


def tn_dot(left, right):
    return lax.dot_general(left, right, (((0,), (0,)), ((), ())), preferred_element_type=f32)


def silu(x):
    return x * (1.0 / (1.0 + jnp.exp(-x)))


def mixer_body(
    in_ref, tx_ref, tb_ref, tc_ref, rate_ref, o_ref, pad_ref, sig_ref, wr_ref, rd_ref, col_ref,
    acc_ref, fwd_ref, bwd_ref,
):
    blocks, tokens, width = o_ref.shape
    groups = width // STATE
    heads = width // HEAD_DIM
    per_group = heads // groups
    taps = tx_ref.shape[0]
    half = taps // 2
    margin = 8
    length = blocks * tokens

    for i in range(3):
        pad_ref[i, :margin] = jnp.zeros((margin, width), f32)
        pad_ref[i, margin + length :] = jnp.zeros((margin, width), f32)

    def widen(c, _):
        for i in range(3):
            pad_ref[i, pl.ds(pl.multiple_of(c * tokens, tokens) + margin, tokens)] = in_ref[
                c, i * tokens : (i + 1) * tokens
            ].astype(f32)
        return 0

    lax.fori_loop(0, blocks, widen, 0)
    fwd_ref[...] = jnp.zeros(fwd_ref.shape, f32)
    bwd_ref[...] = jnp.zeros(bwd_ref.shape, f32)
    row_id = lax.broadcasted_iota(jnp.int32, (tokens, tokens), 0)
    col_id = lax.broadcasted_iota(jnp.int32, (tokens, tokens), 1)
    lower = row_id >= col_id
    upper = row_id <= col_id
    upto = jnp.where(upper, 1.0, 0.0).astype(f32)
    rates = rate_ref[...]
    lane = lax.broadcasted_iota(jnp.int32, (tokens, STATE), 1) // HEAD_DIM

    def conv(i, c, tap_ref):
        window = pad_ref[i, pl.ds(pl.multiple_of(c * tokens, tokens), tokens + 2 * margin)]
        total = window[margin - half : margin - half + tokens] * tap_ref[0:1]
        for j in range(1, taps):
            first = margin - half + j
            total = total + window[first : first + tokens] * tap_ref[j : j + 1]
        return silu(total)

    def spread_heads(cols, g):
        wide = jnp.broadcast_to(cols[g * per_group], (tokens, STATE))
        for k in range(1, per_group):
            wide = jnp.where(
                lane == k, jnp.broadcast_to(cols[g * per_group + k], (tokens, STATE)), wide
            )
        return wide

    def forward(c, _):
        at = pl.ds(pl.multiple_of(c * tokens, tokens), tokens)
        signal = conv(0, c, tx_ref)
        write = conv(1, c, tb_ref).astype(bf16)
        read = conv(2, c, tc_ref).astype(bf16)
        sig_ref[at] = signal
        wr_ref[at] = write
        rd_ref[at] = read
        raw = in_ref[c, 3 * tokens : 3 * tokens + STEP_ROWS, :tokens].astype(f32)
        step = jnp.maximum(raw, 0.0) + jnp.log1p(jnp.exp(-jnp.abs(raw)))
        drop = step * rates
        incl = jnp.dot(drop, upto, precision=highest, preferred_element_type=f32)
        excl = incl - drop
        stacked = jnp.concatenate(
            [incl, excl, step, jnp.zeros((tokens - 3 * STEP_ROWS, tokens), f32)], axis=0
        )
        cols = stacked.T
        col_ref[at] = cols

        def col(kind, row):
            return cols[:, kind * STEP_ROWS + row : kind * STEP_ROWS + row + 1]

        signal_b = signal.astype(bf16)
        reach = [col(0, 2 * h) for h in range(heads)]
        last = [incl[2 * h : 2 * h + 1, tokens - 1 : tokens] for h in range(heads)]
        scale = [col(2, 2 * h) * jnp.exp(reach[h] - last[h]) for h in range(heads)]
        fade = [jnp.exp(-reach[h]) for h in range(heads)]
        keep = [jnp.broadcast_to(jnp.exp(-last[h]), (tokens, 1)) for h in range(heads)]
        for g in range(groups):
            lanes = slice(g * STATE, (g + 1) * STATE)
            read_g = read[:, lanes]
            write_g = write[:, lanes]
            match = nt_dot(read_g, write_g)
            pieces = []
            for h in range(g * per_group, (g + 1) * per_group):
                f, b = 2 * h, 2 * h + 1
                gap = jnp.where(
                    lower, incl[f : f + 1] - reach[h], col(1, b) - excl[b : b + 1]
                )
                weight = jnp.exp(gap) * (
                    jnp.where(lower, step[f : f + 1], 0.0) + jnp.where(upper, step[b : b + 1], 0.0)
                )
                pieces.append(
                    jnp.dot(
                        (match * weight).astype(bf16),
                        signal_b[:, h * HEAD_DIM : (h + 1) * HEAD_DIM],
                        preferred_element_type=f32,
                    )
                )
            state = fwd_ref[g]
            carried = jnp.dot(read_g, state.astype(bf16), preferred_element_type=f32)
            acc_ref[at, lanes] = jnp.concatenate(pieces, axis=1) + carried * spread_heads(fade, g)
            fresh = tn_dot(write_g, (signal[:, lanes] * spread_heads(scale, g)).astype(bf16))
            fwd_ref[g] = state * spread_heads(keep, g) + fresh
        return 0

    lax.fori_loop(0, blocks, forward, 0)

    def backward(i, _):
        c = blocks - 1 - i
        at = pl.ds(pl.multiple_of(c * tokens, tokens), tokens)
        cols = col_ref[at]
        signal = sig_ref[at]
        write = wr_ref[at]
        read = rd_ref[at]

        def col(kind, row):
            return cols[:, kind * STEP_ROWS + row : kind * STEP_ROWS + row + 1]

        ahead = [col(1, 2 * h + 1) for h in range(heads)]
        whole = [col(0, 2 * h + 1)[tokens - 1 : tokens] for h in range(heads)]
        scale = [col(2, 2 * h + 1) * jnp.exp(-ahead[h]) for h in range(heads)]
        fade = [jnp.exp(ahead[h] - whole[h]) for h in range(heads)]
        keep = [jnp.broadcast_to(jnp.exp(-whole[h]), (tokens, 1)) for h in range(heads)]
        for g in range(groups):
            lanes = slice(g * STATE, (g + 1) * STATE)
            state = bwd_ref[g]
            carried = jnp.dot(read[:, lanes], state.astype(bf16), preferred_element_type=f32)
            o_ref[c, :, lanes] = (acc_ref[at, lanes] + carried * spread_heads(fade, g)).astype(bf16)
            fresh = tn_dot(write[:, lanes], (signal[:, lanes] * spread_heads(scale, g)).astype(bf16))
            bwd_ref[g] = state * spread_heads(keep, g) + fresh
        return 0

    lax.fori_loop(0, blocks, backward, 0)


def mixer(arrived, conv_x, conv_b, conv_c, decay_rate):
    blocks, rows, width = arrived.shape
    tokens = (rows - STEP_ROWS) // 3
    length = blocks * tokens
    groups = width // STATE
    rates = decay_rate.T.reshape(-1, 1)
    rates = jnp.pad(rates, ((0, STEP_ROWS - rates.shape[0]), (0, 0)))
    return pl.pallas_call(
        mixer_body,
        out_shape=jax.ShapeDtypeStruct((blocks, tokens, width), bf16),
        scratch_shapes=[
            pltpu.VMEM((3, length + 16, width), f32),
            pltpu.VMEM((length, width), f32),
            pltpu.VMEM((length, width), bf16),
            pltpu.VMEM((length, width), bf16),
            pltpu.VMEM((length, tokens), f32),
            pltpu.VMEM((length, width), f32),
            pltpu.VMEM((groups, STATE, STATE), f32),
            pltpu.VMEM((groups, STATE, STATE), f32),
        ],
        compiler_params=pltpu.CompilerParams(vmem_limit_bytes=32 * 1024 * 1024),
        name="mixer",
    )(arrived, conv_x, conv_b, conv_c, rates)


def project_body(
    mix_ref, gate_ref, gain_ref, w_ref, res_ref, fgain_ref, sel_ref, stream_ref, out_ref, mixed_ref
):
    n = pl.program_id(0)
    parts, tokens, part_width = mix_ref.shape
    model = gate_ref.shape[1]
    span = model // NORM_GROUPS
    each = span // part_width
    block = w_ref.shape[1]

    @pl.when(n == 0)
    def _():
        for q in range(NORM_GROUPS):
            piece = jnp.concatenate([mix_ref[q * each + i] for i in range(each)], axis=1)
            cols = slice(q * span, (q + 1) * span)
            value = piece.astype(f32) * silu(gate_ref[:, cols].astype(f32))
            norm = lax.rsqrt(jnp.mean(value * value, axis=-1, keepdims=True) + epsilon)
            mixed_ref[:, cols] = (value * norm * gain_ref[:, cols]).astype(bf16)

    stream_ref[:, pl.ds(pl.multiple_of(n * block, block), block)] = res_ref[...].astype(
        f32
    ) + jnp.dot(mixed_ref[...], w_ref[...], preferred_element_type=f32)

    @pl.when(n == pl.num_programs(0) - 1)
    def _():
        stream = stream_ref[...]
        norm = lax.rsqrt(jnp.mean(stream * stream, axis=-1, keepdims=True) + epsilon)
        rows = (stream * norm * fgain_ref[...]).astype(bf16)
        out_ref[...] = jnp.dot(sel_ref[...], rows, preferred_element_type=f32).astype(bf16)


def project(mix, gate, gain, weight, residual, fgain, select):
    tokens, model = gate.shape
    block = model // 4
    slots = select.shape[0]

    def whole(shape):
        return pl.BlockSpec(shape, lambda n: (0,) * len(shape))

    return pl.pallas_call(
        project_body,
        grid=(model // block,),
        in_specs=[
            whole(mix.shape),
            whole(gate.shape),
            whole((1, model)),
            pl.BlockSpec((model, block), lambda n: (0, n)),
            pl.BlockSpec((tokens, block), lambda n: (0, n)),
            whole((1, model)),
            whole(select.shape),
        ],
        out_specs=[whole((tokens, model)), whole((slots, model))],
        out_shape=[
            jax.ShapeDtypeStruct((tokens, model), f32),
            jax.ShapeDtypeStruct((slots, model), bf16),
        ],
        scratch_shapes=[pltpu.VMEM((tokens, model), bf16)],
        compiler_params=pltpu.CompilerParams(vmem_limit_bytes=48 * 1024 * 1024),
        name="project",
    )(mix, gate, gain.reshape(1, -1), weight, residual, fgain.reshape(1, -1), select)


def expert_apply(rows, gate_mat, up_mat, down_mat):
    gate_value = jnp.minimum(
        jnp.dot(rows, gate_mat, preferred_element_type=jnp.float32), clamp_limit
    )
    up_value = jnp.clip(
        jnp.dot(rows, up_mat, preferred_element_type=jnp.float32), -clamp_limit, clamp_limit
    )
    active = ((up_value + 1.0) * gate_value * jax.nn.sigmoid(sigmoid_slope * gate_value)).astype(
        jnp.bfloat16
    )
    return jnp.dot(active, down_mat, preferred_element_type=jnp.float32).astype(jnp.bfloat16)


def per_device(
    residual_in,
    ssm_input,
    state_b,
    state_c,
    step_raw,
    gate_input,
    conv_x,
    conv_b,
    conv_c,
    decay_rate,
    mix_gain,
    out_weight,
    ffn_gain,
    routing,
    route_weight,
    gate_w,
    up_w,
    down_w,
):
    sp_count = lax.axis_size("sp")
    dp_count = lax.axis_size("dp")
    experts_all = sp_count * dp_count
    token_count = residual_in.shape[1]
    model_width = residual_in.shape[2]
    top_count = routing.shape[2]
    capacity = 2 * token_count * top_count // experts_all

    steps = step_raw[0].T.reshape(sp_count, -1, token_count)
    steps = jnp.pad(steps, ((0, 0), (0, STEP_ROWS - steps.shape[1]), (0, 0)))
    packed = pack_inputs(ssm_input[0], state_b[0], state_c[0], steps, sp_count)
    arrived_mix = lax.all_to_all(packed, "sp", split_axis=0, concat_axis=0, tiled=True)
    mixed_heads = mixer(arrived_mix, conv_x, conv_b, conv_c, decay_rate)
    mixed_tokens = lax.all_to_all(mixed_heads, "sp", split_axis=0, concat_axis=0, tiled=True)

    routes = routing[0]
    hits = routes.T[:, None, :] == lax.iota(jnp.int32, experts_all)[None, :, None]
    mask = jnp.any(hits, axis=0)
    share = jnp.sum(jnp.where(hits, route_weight[0].T[:, None, :], 0.0), axis=0)
    earlier = (
        lax.iota(jnp.int32, token_count)[:, None] < lax.iota(jnp.int32, token_count)[None, :]
    ).astype(bf16)
    rank = jnp.dot(mask.astype(bf16), earlier, preferred_element_type=f32).astype(jnp.int32)
    rank = jnp.where(mask, rank, capacity)
    chosen = rank[:, None, :] == lax.iota(jnp.int32, capacity)[None, :, None]
    select = chosen.astype(bf16).reshape(experts_all * capacity, token_count)
    share_top = share.astype(bf16)
    share_rest = (share - share_top.astype(f32)).astype(bf16)
    shares = jnp.stack([share_top, share_rest])
    merge = jnp.where(chosen[None], shares[:, :, None, :], jnp.zeros((), bf16)).reshape(
        2, experts_all * capacity, token_count
    )

    stream, outgoing = project(
        mixed_tokens,
        gate_input[0],
        mix_gain,
        lax.all_gather(out_weight, "dp", axis=0, tiled=True),
        residual_in[0],
        ffn_gain,
        select,
    )
    arrived = lax.all_to_all(
        outgoing.reshape(experts_all, capacity, model_width),
        ("sp", "dp"),
        split_axis=0,
        concat_axis=0,
        tiled=True,
    )
    served = expert_apply(arrived.reshape(-1, model_width), gate_w[0], up_w[0], down_w[0]).reshape(
        arrived.shape
    )
    returned = lax.all_to_all(served, ("sp", "dp"), split_axis=0, concat_axis=0, tiled=True)
    routed = jnp.einsum(
        "ast,sd->atd",
        merge,
        returned.reshape(experts_all * capacity, model_width),
        preferred_element_type=f32,
    )
    return (stream + routed[0] + routed[1]).astype(bf16)[None]


def solution(mesh):
    return jax.shard_map(
        per_device,
        mesh=mesh,
        in_specs=(
            P("dp", "sp", None),
            P("dp", "sp", None),
            P("dp", "sp", None),
            P("dp", "sp", None),
            P("dp", "sp", None),
            P("dp", "sp", None),
            P(None, "sp"),
            P(None, "sp"),
            P(None, "sp"),
            P(None, "sp"),
            P(),
            P("dp", None),
            P(),
            P("dp", "sp", None),
            P("dp", "sp", None),
            P(("sp", "dp"), None, None),
            P(("sp", "dp"), None, None),
            P(("sp", "dp"), None, None),
        ),
        out_specs=P("dp", "sp", None),
        check_vma=False,
    )
```

time: 604 us -> 325 us (0.54); the launches traced: 593 us -> 324 us
  other arithmetic: 188 us -> 1.34 us
  local copies, waits for them, and re-layouts: 107 us -> 1.65 us
  waiting for transfers between devices: 101 us -> 147 us
  matrix products: 49.4 us -> 19.9 us
  Pallas kernels: 0 us -> 28.2 us
  starting transfers between devices: 35.4 us -> 14.9 us
    another operation x2 -> x1, other arithmetic: 94.9 us -> 0.01 us  [per_device(): shares = jnp.stack([share_top, share_rest])]
    all_to_all x6 -> x3, waiting for transfers between devices: 100 us -> 147 us  [the longest x1 94.1 us: per_device(): lax.all_to_all(served, ('sp', 'dp'), split_axis=0, concat_axis=0, tiled=T...]
    unnamed x8 -> x0, other arithmetic: 39.5 us -> none
    dot_general x10 -> x2, matrix products: 33.1 us -> 3.59 us  [the longest x1 3.46 us: per_device(): jnp.einsum('ast,sd->atd', merge, returned.reshape(experts_all * capacity,...]
    pallas_call x0 -> x3, Pallas kernels: none -> 28.2 us  [the longest x1 14.1 us: mixer(): pl.pallas_call(mixer_body, out_shape=jax.ShapeDtypeStruct((blocks, tokens...]
    unnamed x95 -> x26, local copies, waits for them, and re-layouts: 22.3 us -> 0.05 us
    rev x5 -> x0, local copies, waits for them, and re-layouts: 21 us -> none  [the longest x1 6.84 us: both_ways(): jnp.flip(write_map, 0)]
    all_to_all x6 -> x3, starting transfers between devices: 35.4 us -> 14.9 us  [the longest x1 7.42 us: per_device(): lax.all_to_all(packed, 'sp', split_axis=0, concat_axis=0, tiled=True)]
  transfers between devices with their start and end apart: 7 -> 4, of which waited for: 3 -> 3; matrix products, arithmetic and copies ran while one was open for 50% -> 1% of each run, Pallas kernels for 0% -> 6%
where the time goes in v1:
time: 325 us; the launch traced here: 324 us
  waiting for transfers between devices  147 us (45%)
  blocking collectives  97.3 us (30%)
  Pallas kernels  28.2 us (9%)
  matrix products  19.9 us (6%)
  starting transfers between devices  14.9 us (5%)
  between operations  13.5 us (4%)
    all_to_all x1, blocking collectives, per_device(): lax.all_to_all(outgoing.reshape(experts_all, capacity, model_width), ('sp...  97.3 us
    all_to_all x1, waiting for transfers between devices, per_device(): lax.all_to_all(served, ('sp', 'dp'), split_axis=0, concat_axis=0, tiled=T...  94.1 us
    all_to_all x1, waiting for transfers between devices, per_device(): lax.all_to_all(packed, 'sp', split_axis=0, concat_axis=0, tiled=True)  38.2 us
    all_to_all x1, waiting for transfers between devices, per_device(): lax.all_to_all(mixed_heads, 'sp', split_axis=0, concat_axis=0, tiled=True)  14.2 us
    pallas_call x1, Pallas kernels, mixer(): pl.pallas_call(mixer_body, out_shape=jax.ShapeDtypeStruct((blocks, tokens...  14.1 us
    pallas_call x1, Pallas kernels, project(): pl.pallas_call(project_body, grid=(model // block,), in_specs=[whole(mix....  8.73 us
    all_to_all x1, starting transfers between devices, per_device(): lax.all_to_all(packed, 'sp', split_axis=0, concat_axis=0, tiled=True)  7.42 us
  transfers between devices with their start and end apart: 4, of which 3 were waited for; matrix products, arithmetic and copies ran while one was open for 1% of the time, Pallas kernels for 6%

profile of v1, /device:TPU:0, one launch (start us, length us, event | category | flops | bytes accessed | tf_op | source)
XLA Modules:
  0.0 324.1 jit_solution(17790503038770481291)
XLA Ops:
  6.5 0.0 all-gather.2.cloned.1.call-start
  6.6 0.7 all-gather.2.cloned.1.call-update
  7.3 1.3 pad.8.s_ref
  8.6 5.4 %pack_inputs.1 = bf16[8,400,256]{2,1,0:T(8,128)(2,1)} custom-call(bf16[128,2048]{1,0:T(8,128)(2,1)} %bitcast.83, bf16[128,2048]{1,0:T(8,128)(2,1)} %bitcast.84, bf16[128,2048]{1,0:T(8,128)(2,1)} %bitcast.85, bf16[8,16,128]{2,1,0:T(8,128)(2,1)} %pad.8.s_ref), custom_call_target="tpu_custom_call" | custom-call | tf_op jit(solution)/shard_map/pack_inputs/pallas_call | solution.py:35
  14.0 7.4 %all-to-all-start = ((bf16[8,400,256]{2,1,0:T(8,128)(2,1)}), bf16[8,400,256]{2,1,0:T(8,128)(2,1)S(1)}, u32[]{:S(2)}, u32[]{:S(2)}) async-start(bf16[8,400,256]{2,1,0:T(8,128)(2,1)} %pack_inputs.1), calls=%async_computation | async-start | bytes 3276800 | tf_op jit(solution)/shard_map/all_to_all | solution.py:325
  21.5 0.1 copy.23
  21.6 0.1 reshape.62
  21.6 38.2 %all-to-all-done.in_ref = bf16[8,400,256]{2,1,0:T(8,128)(2,1)S(1)} async-done(((bf16[8,400,256]{2,1,0:T(8,128)(2,1)}), bf16[8,400,256]{2,1,0:T(8,128)(2,1)S(1)}, u32[]{:S(2)}, u32[]{:S(2)}) %all-to-all-start) | async-done | bytes 1638432 | tf_op jit(solution)/shard_map/all_to_all | solution.py:325
  59.9 14.1 %mixer.1 = bf16[8,128,256]{2,1,0:T(8,128)(2,1)} custom-call(bf16[8,400,256]{2,1,0:T(8,128)(2,1)S(1)} %all-to-all-done.in_ref, f32[7,256]{1,0:T(8,128)S(1)} %copy-done.2, f32[7,256]{1,0:T(8,128)S(1)} %copy-done.3, f32[7,256]{1,0:T(8,128)S(1)} %copy-done.4, f32[16,1]{1,0:T(8,128)S(1)} %pad.9.rate_ref), custom_call_target="tpu_custom_call" | custom-call | tf_op jit(solution)/shard_map/mixer/pallas_call | solution.py:201
  74.0 3.6 %all-to-all-start.1 = ((bf16[8,128,256]{2,1,0:T(8,128)(2,1)}), bf16[8,128,256]{2,1,0:T(8,128)(2,1)S(1)}, u32[]{:S(2)}, u32[]{:S(2)}) async-start(bf16[8,128,256]{2,1,0:T(8,128)(2,1)} %mixer.1), calls=%async_computation.1 | async-start | bytes 1048576 | tf_op jit(solution)/shard_map/all_to_all | solution.py:327
  77.6 0.1 eq.47
  77.7 0.1 fusion.16
  77.9 0.2 fusion.22.sel_ref
  78.1 14.2 %all-to-all-done.1.mix_ref = bf16[8,128,256]{2,1,0:T(8,128)(2,1)S(1)} async-done(((bf16[8,128,256]{2,1,0:T(8,128)(2,1)}), bf16[8,128,256]{2,1,0:T(8,128)(2,1)S(1)}, u32[]{:S(2)}, u32[]{:S(2)}) %all-to-all-start.1) | async-done | bytes 524320 | tf_op jit(solution)/shard_map/all_to_all | solution.py:327
  92.3 8.7 %project.1 = (f32[128,2048]{1,0:T(8,128)S(1)}, bf16[1024,2048]{1,0:T(8,128)(2,1)}) custom-call(bf16[8,128,256]{2,1,0:T(8,128)(2,1)S(1)} %all-to-all-done.1.mix_ref, bf16[128,2048]{1,0:T(8,128)(2,1)S(1)} %bitcast.75, f32[1,2048]{1,0:T(1,128)S(1)} %bitcast.77, bf16[2048,2048]{1,0:T(8,128)(2,1)} %all-gather.2.cloned.1.call-done.w_ref, ...), custom_call_target="tpu_custom_call" | custom-call | tf_op jit(solution)/shard_map/project/pallas_call | solution.py:258
  101.1 97.3 %all_to_all.20 = bf16[32,32,2048]{2,1,0:T(8,128)(2,1)S(1)} all-to-all(bf16[32,32,2048]{2,1,0:T(8,128)(2,1)} %bitcast.80), channel_id=1, replica_groups=mesh['sp'=8,'dp'=4] {'sp','dp'}, dimensions={0} | all-to-all | bytes 8388608 | tf_op jit(solution)/shard_map/all_to_all | solution.py:356
  198.4 4.5 %fusion.4 = f32[1024,1024]{1,0:T(8,128)S(1)} fusion(bf16[1024,2048]{1,0:T(8,128)(2,1)S(1)} %bitcast.81, bf16[1,2048,1024]{2,1,0:T(8,128)(2,1)S(1)} %copy-done.10), kind=kOutput, calls=%fused_computation.4 | convolution fusion | flops 4294967296 | bytes 12582912 | tf_op jit(solution)/shard_map/dot_general | solution.py:283
  202.9 5.7 %multiply_convert_fusion = bf16[1024,1024]{1,0:T(8,128)(2,1)S(1)} fusion(f32[1024,1024]{1,0:T(8,128)S(1)} %fusion.4, bf16[1024,2048]{1,0:T(8,128)(2,1)S(1)} %bitcast.82, bf16[1,2048,1024]{2,1,0:T(8,128)(2,1)S(1)} %copy-done.11), kind=kOutput, calls=%fused_computation.8 | convolution fusion | flops 4305453056 | bytes 14680064 | tf_op jit(solution)/shard_map/dot_general | solution.py:286
  208.6 6.1 %fusion.8 = bf16[1024,2048]{1,0:T(8,128)(2,1)} fusion(bf16[1024,1024]{1,0:T(8,128)(2,1)S(1)} %multiply_convert_fusion, bf16[1,1024,2048]{2,1,0:T(8,128)(2,1)S(1)} %copy-done.12), kind=kOutput, calls=%fused_computation.9 | convolution fusion | flops 4297064448 | bytes 10485760 | tf_op jit(solution)/shard_map/dot_general | solution.py:291
  214.7 3.8 %all-to-all-start.3 = ((bf16[32,32,2048]{2,1,0:T(8,128)(2,1)}), bf16[32,32,2048]{2,1,0:T(8,128)(2,1)}, u32[]{:S(2)}, u32[]{:S(2)}) async-start(bf16[32,32,2048]{2,1,0:T(8,128)(2,1)} %bitcast.79), calls=%async_computation.3 | async-start | bytes 8388608 | tf_op jit(solution)/shard_map/all_to_all | solution.py:366
  218.6 0.1 iota_compare_fusion
  218.7 94.1 %all-to-all-done.3 = bf16[32,32,2048]{2,1,0:T(8,128)(2,1)} async-done(((bf16[32,32,2048]{2,1,0:T(8,128)(2,1)}), bf16[32,32,2048]{2,1,0:T(8,128)(2,1)}, u32[]{:S(2)}, u32[]{:S(2)}) %all-to-all-start.3) | async-done | bytes 4194336 | tf_op jit(solution)/shard_map/all_to_all | solution.py:366
  312.8 3.5 %fusion.11 = f32[2,128,2048]{2,1,0:T(8,128)S(1)} fusion(bf16[32,32,2048]{2,1,0:T(8,128)(2,1)} %all-to-all-done.3, pred[32,32,128]{2,1,0:T(8,128)(4,1)S(1)} %iota_compare_fusion, bf16[2,32,128]{2,1,0:T(8,128)(2,1)S(1)} %pad_maximum_fusion), kind=kOutput, calls=%fused_computation.10 | convolution fusion | flops 1074003968 | bytes 6438912 | tf_op jit(solution)/shard_map/ast,sd->atd/dot_general | solution.py:367
  316.2 1.0 fusion.20
  (33 shorter events, 0.1 us)
Async XLA Ops:
  6.5 14.9 %copy-start.9 = (f32[2,4]{1,0:T(2,128)S(1)}, f32[2,4]{1,0:T(2,128)}, u32[]{:S(2)}) copy-start(f32[2,4]{1,0:T(2,128)} %param.27) | copy-start | bytes 100
  6.5 53.3 %copy-start.2 = (f32[7,256]{1,0:T(8,128)S(1)}, f32[7,256]{1,0:T(8,128)}, u32[]{:S(2)}) copy-start(f32[7,256]{1,0:T(8,128)} %tx_ref.1) | copy-start | bytes 21508
  6.5 53.3 %copy-start.3 = (f32[7,256]{1,0:T(8,128)S(1)}, f32[7,256]{1,0:T(8,128)}, u32[]{:S(2)}) copy-start(f32[7,256]{1,0:T(8,128)} %tb_ref.1) | copy-start | bytes 21508
  6.5 53.3 %copy-start.4 = (f32[7,256]{1,0:T(8,128)S(1)}, f32[7,256]{1,0:T(8,128)}, u32[]{:S(2)}) copy-start(f32[7,256]{1,0:T(8,128)} %tc_ref.1) | copy-start | bytes 21508
  6.5 85.8 %all-gather.2.cloned.1.call-start = ((), (), s32[]{:S(2)}) async-start(), calls=%async_computation.4 | async-start | bytes 10485760 | tf_op jit(solution)/shard_map/all_gather | solution.py:351
  8.6 69.1 %copy-start.7 = (s32[1,128,4]{1,2,0:T(4,128)S(1)}, s32[1,128,4]{1,2,0:T(4,128)}, u32[]{:S(2)}) copy-start(s32[1,128,4]{1,2,0:T(4,128)} %param.31) | copy-start | bytes 6148
  14.0 78.3 %copy-start = (bf16[1,128,2048]{2,1,0:T(8,128)(2,1)S(1)}, bf16[1,128,2048]{2,1,0:T(8,128)(2,1)}, u32[]{:S(2)}) copy-start(bf16[1,128,2048]{2,1,0:T(8,128)(2,1)} %param.23) | copy-start | bytes 1572868
  14.0 78.3 %copy-start.1 = (bf16[1,128,2048]{2,1,0:T(8,128)(2,1)S(1)}, bf16[1,128,2048]{2,1,0:T(8,128)(2,1)}, u32[]{:S(2)}) copy-start(bf16[1,128,2048]{2,1,0:T(8,128)(2,1)} %param.18) | copy-start | bytes 1572868
  14.0 78.3 %copy-start.5 = (f32[2048]{0:T(1024)S(1)}, f32[2048]{0:T(1024)}, u32[]{:S(2)}) copy-start(f32[2048]{0:T(1024)} %param.28) | copy-start | bytes 24580
  14.0 78.3 %copy-start.6 = (f32[2048]{0:T(1024)S(1)}, f32[2048]{0:T(1024)}, u32[]{:S(2)}) copy-start(f32[2048]{0:T(1024)} %param.30) | copy-start | bytes 24580
  14.0 45.8 %all-to-all-start = ((bf16[8,400,256]{2,1,0:T(8,128)(2,1)}), bf16[8,400,256]{2,1,0:T(8,128)(2,1)S(1)}, u32[]{:S(2)}, u32[]{:S(2)}) async-start(bf16[8,400,256]{2,1,0:T(8,128)(2,1)} %pack_inputs.1), calls=%async_computation | async-start | bytes 3276800 | tf_op jit(solution)/shard_map/all_to_all | solution.py:325
  74.0 18.3 %all-to-all-start.1 = ((bf16[8,128,256]{2,1,0:T(8,128)(2,1)}), bf16[8,128,256]{2,1,0:T(8,128)(2,1)S(1)}, u32[]{:S(2)}, u32[]{:S(2)}) async-start(bf16[8,128,256]{2,1,0:T(8,128)(2,1)} %mixer.1), calls=%async_computation.1 | async-start | bytes 1048576 | tf_op jit(solution)/shard_map/all_to_all | solution.py:327
  101.1 97.3 %copy-start.10 = (bf16[1,2048,1024]{2,1,0:T(8,128)(2,1)S(1)}, bf16[1,2048,1024]{2,1,0:T(8,128)(2,1)}, u32[]{:S(2)}) copy-start(bf16[1,2048,1024]{2,1,0:T(8,128)(2,1)} %param.33) | copy-start | bytes 12582916
  198.4 4.5 %copy-start.11 = (bf16[1,2048,1024]{2,1,0:T(8,128)(2,1)S(1)}, bf16[1,2048,1024]{2,1,0:T(8,128)(2,1)}, u32[]{:S(2)}) copy-start(bf16[1,2048,1024]{2,1,0:T(8,128)(2,1)} %param.34) | copy-start | bytes 12582916
  202.9 5.7 %copy-start.12 = (bf16[1,1024,2048]{2,1,0:T(8,128)(2,1)S(1)}, bf16[1,1024,2048]{2,1,0:T(8,128)(2,1)}, u32[]{:S(2)}) copy-start(bf16[1,1024,2048]{2,1,0:T(8,128)(2,1)} %param.35) | copy-start | bytes 12582916
  214.7 3.8 %copy-start.8 = (f32[1,128,4]{1,2,0:T(4,128)S(1)}, f32[1,128,4]{1,2,0:T(4,128)}, u32[]{:S(2)}) copy-start(f32[1,128,4]{1,2,0:T(4,128)} %param.32) | copy-start | bytes 6148
  214.7 98.0 %all-to-all-start.3 = ((bf16[32,32,2048]{2,1,0:T(8,128)(2,1)}), bf16[32,32,2048]{2,1,0:T(8,128)(2,1)}, u32[]{:S(2)}, u32[]{:S(2)}) async-start(bf16[32,32,2048]{2,1,0:T(8,128)(2,1)} %bitcast.79), calls=%async_computation.3 | async-start | bytes 8388608 | tf_op jit(solution)/shard_map/all_to_all | solution.py:366
Sparse Core Ops, SparseCore 0:
  8.9 60.9 all-gather.1

commit v2 on v1

--- a/solution.py
+++ b/solution.py
@@ -216,15 +216,16 @@
     )(arrived, conv_x, conv_b, conv_c, rates)
 
 
-def project_body(
-    mix_ref, gate_ref, gain_ref, w_ref, res_ref, fgain_ref, sel_ref, stream_ref, out_ref, mixed_ref
-):
+def project_body(place_ref, mix_ref, gate_ref, gain_ref, res_ref, fgain_ref, *rest):
+    *w_refs, stream_ref, rows_ref, mixed_ref = rest
     n = pl.program_id(0)
     parts, tokens, part_width = mix_ref.shape
     model = gate_ref.shape[1]
     span = model // NORM_GROUPS
     each = span // part_width
-    block = w_ref.shape[1]
+    seg = mixed_ref.shape[2]
+    unit = min(seg, span)
+    block = w_refs[0].shape[1]
 
     @pl.when(n == 0)
     def _():
@@ -233,24 +234,30 @@
             cols = slice(q * span, (q + 1) * span)
             value = piece.astype(f32) * silu(gate_ref[:, cols].astype(f32))
             norm = lax.rsqrt(jnp.mean(value * value, axis=-1, keepdims=True) + epsilon)
-            mixed_ref[:, cols] = (value * norm * gain_ref[:, cols]).astype(bf16)
-
-    stream_ref[:, pl.ds(pl.multiple_of(n * block, block), block)] = res_ref[...].astype(
-        f32
-    ) + jnp.dot(mixed_ref[...], w_ref[...], preferred_element_type=f32)
+            value = (value * norm * gain_ref[:, cols]).astype(bf16)
+            for u in range(0, span, unit):
+                at = q * span + u
+                mixed_ref[at // seg, :, at % seg : at % seg + unit] = value[:, u : u + unit]
+
+    total = res_ref[...].astype(f32)
+    for m in range(len(w_refs)):
+        total = total + jnp.dot(
+            mixed_ref[place_ref[0] ^ m], w_refs[m][...], preferred_element_type=f32
+        )
+    stream_ref[:, pl.ds(pl.multiple_of(n * block, block), block)] = total
 
     @pl.when(n == pl.num_programs(0) - 1)
     def _():
         stream = stream_ref[...]
         norm = lax.rsqrt(jnp.mean(stream * stream, axis=-1, keepdims=True) + epsilon)
         rows = (stream * norm * fgain_ref[...]).astype(bf16)
-        out_ref[...] = jnp.dot(sel_ref[...], rows, preferred_element_type=f32).astype(bf16)
-
-
-def project(mix, gate, gain, weight, residual, fgain, select):
+        rows_ref[...] = rows
+
+
+def project(place, mix, gate, gain, weights, residual, fgain):
     tokens, model = gate.shape
     block = model // 4
-    slots = select.shape[0]
+    seg = weights[0].shape[0]
 
     def whole(shape):
         return pl.BlockSpec(shape, lambda n: (0,) * len(shape))
@@ -259,23 +266,49 @@
         project_body,
         grid=(model // block,),
         in_specs=[
+            pl.BlockSpec(memory_space=pltpu.SMEM),
             whole(mix.shape),
             whole(gate.shape),
             whole((1, model)),
-            pl.BlockSpec((model, block), lambda n: (0, n)),
             pl.BlockSpec((tokens, block), lambda n: (0, n)),
             whole((1, model)),
-            whole(select.shape),
-        ],
-        out_specs=[whole((tokens, model)), whole((slots, model))],
+        ]
+        + [pl.BlockSpec((seg, block), lambda n: (0, n))] * len(weights),
+        out_specs=[whole((tokens, model)), whole((tokens, model))],
         out_shape=[
             jax.ShapeDtypeStruct((tokens, model), f32),
-            jax.ShapeDtypeStruct((slots, model), bf16),
+            jax.ShapeDtypeStruct((tokens, model), bf16),
         ],
-        scratch_shapes=[pltpu.VMEM((tokens, model), bf16)],
+        scratch_shapes=[pltpu.VMEM((model // seg, tokens, seg), bf16)],
         compiler_params=pltpu.CompilerParams(vmem_limit_bytes=48 * 1024 * 1024),
         name="project",
-    )(mix, gate, gain.reshape(1, -1), weight, residual, fgain.reshape(1, -1), select)
+    )(place, mix, gate, gain.reshape(1, -1), residual, fgain.reshape(1, -1), *weights)
+
+
+def slot_maps(routes, weights, first, experts, capacity):
+    tokens = routes.shape[0]
+    hits = routes.T[:, None, :] == (first + lax.iota(jnp.int32, experts))[None, :, None]
+    mask = jnp.any(hits, axis=0)
+    share = jnp.sum(jnp.where(hits, weights.T[:, None, :], 0.0), axis=0)
+    earlier = (lax.iota(jnp.int32, tokens)[:, None] < lax.iota(jnp.int32, tokens)[None, :]).astype(
+        bf16
+    )
+    rank = jnp.dot(mask.astype(bf16), earlier, preferred_element_type=f32).astype(jnp.int32)
+    rank = jnp.where(mask, rank, capacity)
+    chosen = rank[:, None, :] == lax.iota(jnp.int32, capacity)[None, :, None]
+    select = chosen.astype(bf16).reshape(experts * capacity, tokens)
+    share_top = share.astype(bf16)
+    share_rest = (share - share_top.astype(f32)).astype(bf16)
+    shares = jnp.stack([share_top, share_rest])
+    merge = jnp.where(chosen[None], shares[:, :, None, :], jnp.zeros((), bf16)).reshape(
+        2, experts * capacity, tokens
+    )
+    return select, merge
+
+
+def weighted_sum(merge, answers):
+    both = jnp.einsum("ast,sd->atd", merge, answers, preferred_element_type=f32)
+    return both[0] + both[1]
 
 
 def expert_apply(rows, gate_mat, up_mat, down_mat):
@@ -311,92 +344,106 @@
     up_w,
     down_w,
 ):
-    sp_count = lax.axis_size("sp")
+    sp_axes = ("half", "rest")
+    group_axes = ("rest", "dp")
+    sp_count = lax.axis_size(sp_axes)
     dp_count = lax.axis_size("dp")
+    group = lax.axis_size(group_axes)
     experts_all = sp_count * dp_count
     token_count = residual_in.shape[1]
     model_width = residual_in.shape[2]
     top_count = routing.shape[2]
     capacity = 2 * token_count * top_count // experts_all
+    swap = [(0, 1), (1, 0)]
+
+    pieces = {0: out_weight}
+    bit = dp_count // 2
+    while bit:
+        steps_of = [(i, i ^ bit) for i in range(dp_count)]
+        fresh = {m ^ bit: lax.ppermute(piece, "dp", steps_of) for m, piece in pieces.items()}
+        pieces.update(fresh)
+        bit //= 2
+
+    other_routes = lax.ppermute(routing[0], "half", swap)
+    other_weight = lax.ppermute(route_weight[0], "half", swap)
 
     steps = step_raw[0].T.reshape(sp_count, -1, token_count)
     steps = jnp.pad(steps, ((0, 0), (0, STEP_ROWS - steps.shape[1]), (0, 0)))
     packed = pack_inputs(ssm_input[0], state_b[0], state_c[0], steps, sp_count)
-    arrived_mix = lax.all_to_all(packed, "sp", split_axis=0, concat_axis=0, tiled=True)
+    arrived_mix = lax.all_to_all(packed, sp_axes, split_axis=0, concat_axis=0, tiled=True)
+    arrived_mix, other_routes, other_weight = lax.optimization_barrier(
+        (arrived_mix, other_routes, other_weight)
+    )
     mixed_heads = mixer(arrived_mix, conv_x, conv_b, conv_c, decay_rate)
-    mixed_tokens = lax.all_to_all(mixed_heads, "sp", split_axis=0, concat_axis=0, tiled=True)
-
-    routes = routing[0]
-    hits = routes.T[:, None, :] == lax.iota(jnp.int32, experts_all)[None, :, None]
-    mask = jnp.any(hits, axis=0)
-    share = jnp.sum(jnp.where(hits, route_weight[0].T[:, None, :], 0.0), axis=0)
-    earlier = (
-        lax.iota(jnp.int32, token_count)[:, None] < lax.iota(jnp.int32, token_count)[None, :]
-    ).astype(bf16)
-    rank = jnp.dot(mask.astype(bf16), earlier, preferred_element_type=f32).astype(jnp.int32)
-    rank = jnp.where(mask, rank, capacity)
-    chosen = rank[:, None, :] == lax.iota(jnp.int32, capacity)[None, :, None]
-    select = chosen.astype(bf16).reshape(experts_all * capacity, token_count)
-    share_top = share.astype(bf16)
-    share_rest = (share - share_top.astype(f32)).astype(bf16)
-    shares = jnp.stack([share_top, share_rest])
-    merge = jnp.where(chosen[None], shares[:, :, None, :], jnp.zeros((), bf16)).reshape(
-        2, experts_all * capacity, token_count
-    )
-
-    stream, outgoing = project(
+    mixed_tokens = lax.all_to_all(mixed_heads, sp_axes, split_axis=0, concat_axis=0, tiled=True)
+
+    first = lax.axis_index("half") * group
+    select, merge = slot_maps(routing[0], route_weight[0], first, group, capacity)
+    other_select, other_merge = slot_maps(other_routes, other_weight, first, group, capacity)
+
+    stream, rows = project(
+        lax.axis_index("dp").reshape(1),
         mixed_tokens,
         gate_input[0],
         mix_gain,
-        lax.all_gather(out_weight, "dp", axis=0, tiled=True),
+        [pieces[m] for m in range(dp_count)],
         residual_in[0],
         ffn_gain,
-        select,
-    )
-    arrived = lax.all_to_all(
-        outgoing.reshape(experts_all, capacity, model_width),
-        ("sp", "dp"),
-        split_axis=0,
-        concat_axis=0,
-        tiled=True,
-    )
-    served = expert_apply(arrived.reshape(-1, model_width), gate_w[0], up_w[0], down_w[0]).reshape(
-        arrived.shape
-    )
-    returned = lax.all_to_all(served, ("sp", "dp"), split_axis=0, concat_axis=0, tiled=True)
-    routed = jnp.einsum(
-        "ast,sd->atd",
-        merge,
-        returned.reshape(experts_all * capacity, model_width),
-        preferred_element_type=f32,
-    )
-    return (stream + routed[0] + routed[1]).astype(bf16)[None]
+    )
+
+    def exchange(slots):
+        return lax.all_to_all(
+            slots.reshape(group, capacity, model_width),
+            group_axes,
+            split_axis=0,
+            concat_axis=0,
+            tiled=True,
+        ).reshape(group * capacity, model_width)
+
+    other_rows = lax.ppermute(rows, "half", swap)
+    arrived = exchange(jnp.dot(select, rows, preferred_element_type=f32).astype(bf16))
+    other_rows, arrived = lax.optimization_barrier((other_rows, arrived))
+    other_arrived = exchange(
+        jnp.dot(other_select, other_rows, preferred_element_type=f32).astype(bf16)
+    )
+    served = expert_apply(arrived, gate_w[0], up_w[0], down_w[0])
+    other_served = expert_apply(other_arrived, gate_w[0], up_w[0], down_w[0])
+    other_answers = exchange(other_served)
+    other_sum = weighted_sum(other_merge, other_answers).astype(bf16)
+    served, other_sum = lax.optimization_barrier((served, other_sum))
+    from_other = lax.ppermute(other_sum, "half", swap)
+    answers = exchange(served)
+    return (stream + weighted_sum(merge, answers) + from_other.astype(f32)).astype(bf16)[None]
 
 
 def solution(mesh):
+    devices = mesh.devices
+    halves = jax.sharding.Mesh(
+        devices.reshape(2, devices.shape[0] // 2, devices.shape[1]), ("half", "rest", "dp")
+    )
     return jax.shard_map(
         per_device,
-        mesh=mesh,
+        mesh=halves,
         in_specs=(
-            P("dp", "sp", None),
-            P("dp", "sp", None),
-            P("dp", "sp", None),
-            P("dp", "sp", None),
-            P("dp", "sp", None),
-            P("dp", "sp", None),
-            P(None, "sp"),
-            P(None, "sp"),
-            P(None, "sp"),
-            P(None, "sp"),
+            P("dp", ("half", "rest"), None),
+            P("dp", ("half", "rest"), None),
+            P("dp", ("half", "rest"), None),
+            P("dp", ("half", "rest"), None),
+            P("dp", ("half", "rest"), None),
+            P("dp", ("half", "rest"), None),
+            P(None, ("half", "rest")),
+            P(None, ("half", "rest")),
+            P(None, ("half", "rest")),
+            P(None, ("half", "rest")),
             P(),
             P("dp", None),
             P(),
-            P("dp", "sp", None),
-            P("dp", "sp", None),
-            P(("sp", "dp"), None, None),
-            P(("sp", "dp"), None, None),
-            P(("sp", "dp"), None, None),
+            P("dp", ("half", "rest"), None),
+            P("dp", ("half", "rest"), None),
+            P(("half", "rest", "dp"), None, None),
+            P(("half", "rest", "dp"), None, None),
+            P(("half", "rest", "dp"), None, None),
         ),
-        out_specs=P("dp", "sp", None),
+        out_specs=P("dp", ("half", "rest"), None),
         check_vma=False,
     )

time: 325 us -> 272 us (0.84)
  blocking collectives: 97.3 us -> 31.9 us
  matrix products: 19.9 us -> 39.8 us
  starting transfers between devices: 14.9 us -> 32.2 us
  between operations: 13.5 us -> 0.24 us
  waiting for transfers between devices: 147 us -> 136 us
  Pallas kernels: 28.2 us -> 24.6 us
    all_to_all x3 -> x5, waiting for transfers between devices: 147 us -> 64.3 us  [the longest x3 51.2 us: exchange(): lax.all_to_all(slots.reshape(group, capacity, model_width), group_axes, s...]
    ppermute x0 -> x7, waiting for transfers between devices: none -> 72.1 us  [the longest x1 34.8 us: per_device(): other_rows = lax.ppermute(rows, 'half', swap)]
    all_to_all x1, blocking collectives: 97.3 us -> 31.9 us  [exchange(): lax.all_to_all(slots.reshape(group, capacity, model_width), group_axes, s...]
    dot_general x1 -> x2, matrix products: 6.13 us -> 22 us  [expert_apply(): jnp.dot(active, down_mat, preferred_element_type=jnp.float32)]
    ppermute x0 -> x7, starting transfers between devices: none -> 8.96 us  [the longest x3 3.07 us: per_device(): lax.ppermute(piece, 'dp', steps_of)]
    all_to_all x3 -> x5, starting transfers between devices: 14.9 us -> 23.2 us  [the longest x3 13.5 us: exchange(): lax.all_to_all(slots.reshape(group, capacity, model_width), group_axes, s...]
    dot_general x1 -> x2, matrix products: 5.66 us -> 10.2 us  [expert_apply(): jnp.dot(rows, up_mat, preferred_element_type=jnp.float32)]
    pallas_call x1, Pallas kernels: 8.73 us -> 5.13 us  [project(): pl.pallas_call(project_body, grid=(model // block,), in_specs=[pl.BlockSp...]
  transfers between devices with their start and end apart: 4 -> 12, of which waited for: 3 -> 8; matrix products, arithmetic and copies ran while one was open for 1% -> 8% of each run, Pallas kernels for 6% -> 7%
where the time goes in v2:
time: 272 us
  waiting for transfers between devices  136 us (50%)
  matrix products  39.8 us (15%)
  starting transfers between devices  32.2 us (12%)
  blocking collectives  31.9 us (12%)
  Pallas kernels  24.6 us (9%)
  local copies, waits for them, and re-layouts  4.62 us (2%)
    all_to_all x3, waiting for transfers between devices, exchange(): lax.all_to_all(slots.reshape(group, capacity, model_width), group_axes, s...  51.2 us
    ppermute x1, waiting for transfers between devices, per_device(): other_rows = lax.ppermute(rows, 'half', swap)  34.8 us
    ppermute x3, waiting for transfers between devices, per_device(): lax.ppermute(piece, 'dp', steps_of)  33.1 us
    all_to_all x1, blocking collectives, exchange(): lax.all_to_all(slots.reshape(group, capacity, model_width), group_axes, s...  31.9 us
    dot_general x2, matrix products, expert_apply(): jnp.dot(active, down_mat, preferred_element_type=jnp.float32)  22 us
    pallas_call x1, Pallas kernels, mixer(): pl.pallas_call(mixer_body, out_shape=jax.ShapeDtypeStruct((blocks, tokens...  14.1 us
    all_to_all x3, starting transfers between devices, exchange(): lax.all_to_all(slots.reshape(group, capacity, model_width), group_axes, s...  13.5 us
    all_to_all x1, waiting for transfers between devices, per_device(): lax.all_to_all(mixed_heads, sp_axes, split_axis=0, concat_axis=0, tiled=T...  13.1 us
  transfers between devices with their start and end apart: 12, of which 8 were waited for; matrix products, arithmetic and copies ran while one was open for 8% of the time, Pallas kernels for 7%

profile of v2, /device:TPU:0, one launch (start us, length us, event | category | flops | bytes accessed | tf_op | source)
XLA Modules:
  0.0 271.5 jit_solution(17284751317567366281)
XLA Ops:
  0.0 3.0 %collective-permute-start.3 = (bf16[512,2048]{1,0:T(8,128)(2,1)}, bf16[512,2048]{1,0:T(8,128)(2,1)}, u32[]{:S(2)}, u32[]{:S(2)}) collective-permute-start(bf16[512,2048]{1,0:T(8,128)(2,1)} %rest_0_.1), channel_id=1, source_target_pairs={{0,2},{1,3},{2,0},{3,1},{4,6},{5,7},{6,4},{7,5},{8,10},{9,11},{10,... | collective-permute-start | bytes 6291464 | tf_op jit(solution)/shard_map/ppermute | solution.py:363
  4.3 5.4 %pack_inputs.1 = bf16[8,400,256]{2,1,0:T(8,128)(2,1)} custom-call(bf16[128,2048]{1,0:T(8,128)(2,1)} %bitcast.117, bf16[128,2048]{1,0:T(8,128)(2,1)} %bitcast.118, bf16[128,2048]{1,0:T(8,128)(2,1)} %bitcast.119, bf16[8,16,128]{2,1,0:T(8,128)(2,1)} %pad.8.s_ref), custom_call_target="tpu_custom_call" | custom-call | tf_op jit(solution)/shard_map/pack_inputs/pallas_call | solution.py:35
  9.8 5.9 %all-to-all-start = ((bf16[8,400,256]{2,1,0:T(8,128)(2,1)}), bf16[8,400,256]{2,1,0:T(8,128)(2,1)S(1)}, u32[]{:S(2)}, u32[]{:S(2)}) async-start(bf16[8,400,256]{2,1,0:T(8,128)(2,1)} %pack_inputs.1), calls=%async_computation | async-start | bytes 3276800 | tf_op jit(solution)/shard_map/all_to_all | solution.py:373
  15.8 33.1 %collective-permute-done.3.rest_2_ = bf16[512,2048]{1,0:T(8,128)(2,1)} collective-permute-done((bf16[512,2048]{1,0:T(8,128)(2,1)}, bf16[512,2048]{1,0:T(8,128)(2,1)}, u32[]{:S(2)}, u32[]{:S(2)}) %collective-permute-start.3) | collective-permute-done | bytes 2097184 | tf_op jit(solution)/shard_map/ppermute | solution.py:363
  48.9 2.8 %collective-permute-start = (s32[128,4]{0,1:T(4,128)S(1)}, s32[128,4]{0,1:T(4,128)S(1)}, u32[]{:S(2)}, u32[]{:S(2)}) collective-permute-start(s32[128,4]{0,1:T(4,128)S(1)} %bitcast.121), channel_id=1, source_target_pairs={{0,16},{16,0},{1,17},{17,1},{2,18},{18,2},{3,19},{19,3},{4,20},{20... | collective-permute-start | bytes 6152 | tf_op jit(solution)/shard_map/ppermute | solution.py:367
  53.9 2.4 collective-permute-done.1
  56.3 14.1 %mixer.1 = bf16[8,128,256]{2,1,0:T(8,128)(2,1)} custom-call(bf16[8,400,256]{2,1,0:T(8,128)(2,1)S(1)} %all-to-all-done.in_ref, f32[7,256]{1,0:T(8,128)S(1)} %copy-done.3, f32[7,256]{1,0:T(8,128)S(1)} %copy-done.4, f32[7,256]{1,0:T(8,128)S(1)} %copy-done.5, f32[16,1]{1,0:T(8,128)S(1)} %pad.9.rate_ref), custom_call_target="tpu_custom_call" | custom-call | tf_op jit(solution)/shard_map/mixer/pallas_call | solution.py:201
  70.4 3.8 %all-to-all-start.1 = ((bf16[8,128,256]{2,1,0:T(8,128)(2,1)}), bf16[8,128,256]{2,1,0:T(8,128)(2,1)S(1)}, u32[]{:S(2)}, u32[]{:S(2)}) async-start(bf16[8,128,256]{2,1,0:T(8,128)(2,1)} %mixer.1), calls=%async_computation.1 | async-start | bytes 1048576 | tf_op jit(solution)/shard_map/all_to_all | solution.py:378
  74.8 13.1 %all-to-all-done.1.mix_ref = bf16[8,128,256]{2,1,0:T(8,128)(2,1)S(1)} async-done(((bf16[8,128,256]{2,1,0:T(8,128)(2,1)}), bf16[8,128,256]{2,1,0:T(8,128)(2,1)S(1)}, u32[]{:S(2)}, u32[]{:S(2)}) %all-to-all-start.1) | async-done | bytes 524320 | tf_op jit(solution)/shard_map/all_to_all | solution.py:378
  89.6 5.1 %project.1 = (f32[128,2048]{1,0:T(8,128)S(1)}, bf16[128,2048]{1,0:T(8,128)(2,1)S(1)}) custom-call(s32[1]{0:T(128)} %bitcast.place_ref, bf16[8,128,256]{2,1,0:T(8,128)(2,1)S(1)} %all-to-all-done.1.mix_ref, bf16[128,2048]{1,0:T(8,128)(2,1)S(1)} %bitcast.107, f32[1,2048]{1,0:T(1,128)S(1)} %bitcast.109, bf16[128,2048]{1,0:T(8,128)(2,1)S(1)} %bitcast.108, ...), custom_call_target="tpu_custom_call" | custom-call | tf_op jit(solution)/shard_map/project/pallas_call | solution.py:265
  96.7 4.4 %all-to-all-start.2 = ((bf16[16,32,2048]{2,1,0:T(8,128)(2,1)}), bf16[16,32,2048]{2,1,0:T(8,128)(2,1)}, u32[]{:S(2)}, u32[]{:S(2)}) async-start(bf16[16,32,2048]{2,1,0:T(8,128)(2,1)} %bitcast.111), calls=%async_computation.2 | async-start | bytes 4194304 | tf_op jit(solution)/shard_map/all_to_all | solution.py:395
  102.1 34.8 %collective-permute-done.5 = bf16[128,2048]{1,0:T(8,128)(2,1)S(1)} collective-permute-done((bf16[128,2048]{1,0:T(8,128)(2,1)S(1)}, bf16[128,2048]{1,0:T(8,128)(2,1)S(1)}, u32[]{:S(2)}, u32[]{:S(2)}) %collective-permute-start.5) | collective-permute-done | bytes 524320 | tf_op jit(solution)/shard_map/ppermute | solution.py:403
  136.9 2.9 %all-to-all-done.2 = bf16[16,32,2048]{2,1,0:T(8,128)(2,1)} async-done(((bf16[16,32,2048]{2,1,0:T(8,128)(2,1)}), bf16[16,32,2048]{2,1,0:T(8,128)(2,1)}, u32[]{:S(2)}, u32[]{:S(2)}) %all-to-all-start.2) | async-done | bytes 2097184 | tf_op jit(solution)/shard_map/all_to_all | solution.py:395
  140.5 31.9 %all_to_all.30 = bf16[16,32,2048]{2,1,0:T(8,128)(2,1)S(1)} all-to-all(bf16[16,32,2048]{2,1,0:T(8,128)(2,1)S(1)} %bitcast.112), channel_id=1, replica_groups=mesh['half'=2,'rest'=4,'dp'=4] {'rest','dp'}, dimensions={0} | all-to-all | bytes 4194304 | tf_op jit(solution)/shard_map/all_to_all | solution.py:395
  173.8 3.7 %fusion.8 = f32[512,1024]{1,0:T(8,128)} fusion(bf16[512,2048]{1,0:T(8,128)(2,1)S(1)} %bitcast.115, bf16[1,2048,1024]{2,1,0:T(8,128)(2,1)S(1)} %copy-done.12), kind=kOutput, calls=%fused_computation.8 | convolution fusion | flops 2147483648 | bytes 8388608 | tf_op jit(solution)/shard_map/dot_general | solution.py:319
  177.5 10.9 %fusion.15 = bf16[512,2048]{1,0:T(8,128)(2,1)} fusion(bf16[1,1024,2048]{2,1,0:T(8,128)(2,1)} %param.35, f32[512,1024]{1,0:T(8,128)} %fusion.8, bf16[512,2048]{1,0:T(8,128)(2,1)} %bitcast.116, bf16[1,2048,1024]{2,1,0:T(8,128)(2,1)} %param.33), kind=kOutput, calls=%fused_computation.13 | convolution fusion | flops 4301258752 | bytes 14680064 | tf_op jit(solution)/shard_map/dot_general | solution.py:324
  188.4 4.6 %all-to-all-start.4 = ((bf16[16,32,2048]{2,1,0:T(8,128)(2,1)}), bf16[16,32,2048]{2,1,0:T(8,128)(2,1)}, u32[]{:S(2)}, u32[]{:S(2)}) async-start(bf16[16,32,2048]{2,1,0:T(8,128)(2,1)} %bitcast.113), calls=%async_computation.4 | async-start | bytes 4194304 | tf_op jit(solution)/shard_map/all_to_all | solution.py:395
  193.2 6.6 %fusion.10 = f32[512,1024]{1,0:T(8,128)} fusion(bf16[512,2048]{1,0:T(8,128)(2,1)} %bitcast.19, bf16[1,2048,1024]{2,1,0:T(8,128)(2,1)} %param.34), kind=kOutput, calls=%fused_computation.10 | convolution fusion | flops 2147483648 | bytes 8388608 | tf_op jit(solution)/shard_map/dot_general | solution.py:319
  199.7 11.0 %fusion.12 = bf16[512,2048]{1,0:T(8,128)(2,1)} fusion(bf16[1,1024,2048]{2,1,0:T(8,128)(2,1)} %param.35, f32[512,1024]{1,0:T(8,128)} %fusion.10, bf16[512,2048]{1,0:T(8,128)(2,1)} %bitcast.19, bf16[1,2048,1024]{2,1,0:T(8,128)(2,1)} %param.33), kind=kOutput, calls=%fused_computation.12 | convolution fusion | flops 4301258752 | bytes 14680064 | tf_op jit(solution)/shard_map/dot_general | solution.py:324
  210.8 11.8 %all-to-all-done.4 = bf16[16,32,2048]{2,1,0:T(8,128)(2,1)} async-done(((bf16[16,32,2048]{2,1,0:T(8,128)(2,1)}), bf16[16,32,2048]{2,1,0:T(8,128)(2,1)}, u32[]{:S(2)}, u32[]{:S(2)}) %all-to-all-start.4) | async-done | bytes 2097184 | tf_op jit(solution)/shard_map/all_to_all | solution.py:395
  222.5 2.3 convolution_bitcast_fusion.1
  225.0 4.5 %all-to-all-start.5 = ((bf16[16,32,2048]{2,1,0:T(8,128)(2,1)}), bf16[16,32,2048]{2,1,0:T(8,128)(2,1)}, u32[]{:S(2)}, u32[]{:S(2)}) async-start(bf16[16,32,2048]{2,1,0:T(8,128)(2,1)} %bitcast.114), calls=%async_computation.5 | async-start | bytes 4194304 | tf_op jit(solution)/shard_map/all_to_all | solution.py:395
  231.5 36.5 %all-to-all-done.5 = bf16[16,32,2048]{2,1,0:T(8,128)(2,1)} async-done(((bf16[16,32,2048]{2,1,0:T(8,128)(2,1)}), bf16[16,32,2048]{2,1,0:T(8,128)(2,1)}, u32[]{:S(2)}, u32[]{:S(2)}) %all-to-all-start.5) | async-done | bytes 2097184 | tf_op jit(solution)/shard_map/all_to_all | solution.py:395
  268.1 2.3 convolution_bitcast_fusion
  (57 shorter events, 14.2 us)
Async XLA Ops:
  0.0 48.9 %collective-permute-start.3 = (bf16[512,2048]{1,0:T(8,128)(2,1)}, bf16[512,2048]{1,0:T(8,128)(2,1)}, u32[]{:S(2)}, u32[]{:S(2)}) collective-permute-start(bf16[512,2048]{1,0:T(8,128)(2,1)} %rest_0_.1), channel_id=1, source_target_pairs={{0,2},{1,3},{2,0},{3,1},{4,6},{5,7},{6,4},{7,5},{8,10},{9,11},{10,... | collective-permute-start | bytes 6291464 | tf_op jit(solution)/shard_map/ppermute | solution.py:363
  9.7 39.2 %copy-start.9 = (s32[1,128,4]{1,2,0:T(4,128)S(1)}, s32[1,128,4]{1,2,0:T(4,128)}, u32[]{:S(2)}) copy-start(s32[1,128,4]{1,2,0:T(4,128)} %param.31) | copy-start | bytes 6148
  9.7 42.1 %copy-start.10 = (f32[1,128,4]{1,2,0:T(4,128)S(1)}, f32[1,128,4]{1,2,0:T(4,128)}, u32[]{:S(2)}) copy-start(f32[1,128,4]{1,2,0:T(4,128)} %param.32) | copy-start | bytes 6148
  9.7 42.2 %copy-start.11 = (f32[2,4]{1,0:T(2,128)S(1)}, f32[2,4]{1,0:T(2,128)}, u32[]{:S(2)}) copy-start(f32[2,4]{1,0:T(2,128)} %param.27) | copy-start | bytes 100
  9.7 46.5 %copy-start.3 = (f32[7,256]{1,0:T(8,128)S(1)}, f32[7,256]{1,0:T(8,128)}, u32[]{:S(2)}) copy-start(f32[7,256]{1,0:T(8,128)} %tx_ref.1) | copy-start | bytes 21508
  9.7 46.5 %copy-start.4 = (f32[7,256]{1,0:T(8,128)S(1)}, f32[7,256]{1,0:T(8,128)}, u32[]{:S(2)}) copy-start(f32[7,256]{1,0:T(8,128)} %tb_ref.1) | copy-start | bytes 21508
  9.7 46.5 %copy-start.5 = (f32[7,256]{1,0:T(8,128)S(1)}, f32[7,256]{1,0:T(8,128)}, u32[]{:S(2)}) copy-start(f32[7,256]{1,0:T(8,128)} %tc_ref.1) | copy-start | bytes 21508
  9.8 46.5 %all-to-all-start = ((bf16[8,400,256]{2,1,0:T(8,128)(2,1)}), bf16[8,400,256]{2,1,0:T(8,128)(2,1)S(1)}, u32[]{:S(2)}, u32[]{:S(2)}) async-start(bf16[8,400,256]{2,1,0:T(8,128)(2,1)} %pack_inputs.1), calls=%async_computation | async-start | bytes 3276800 | tf_op jit(solution)/shard_map/all_to_all | solution.py:373
  15.7 72.3 %copy-start.1 = (bf16[1,128,2048]{2,1,0:T(8,128)(2,1)S(1)}, bf16[1,128,2048]{2,1,0:T(8,128)(2,1)}, u32[]{:S(2)}) copy-start(bf16[1,128,2048]{2,1,0:T(8,128)(2,1)} %param.23) | copy-start | bytes 1572868
  15.7 72.3 %copy-start.2 = (bf16[1,128,2048]{2,1,0:T(8,128)(2,1)S(1)}, bf16[1,128,2048]{2,1,0:T(8,128)(2,1)}, u32[]{:S(2)}) copy-start(bf16[1,128,2048]{2,1,0:T(8,128)(2,1)} %param.18) | copy-start | bytes 1572868
  15.7 72.2 %copy-start.6 = (f32[2048]{0:T(1024)S(1)}, f32[2048]{0:T(1024)}, u32[]{:S(2)}) copy-start(f32[2048]{0:T(1024)} %param.28) | copy-start | bytes 24580
  15.7 72.2 %copy-start.7 = (f32[2048]{0:T(1024)S(1)}, f32[2048]{0:T(1024)}, u32[]{:S(2)}) copy-start(f32[2048]{0:T(1024)} %param.30) | copy-start | bytes 24580
  15.7 59.1 %collective-permute-start.2 = (bf16[512,2048]{1,0:T(8,128)(2,1)}, bf16[512,2048]{1,0:T(8,128)(2,1)}, u32[]{:S(2)}, u32[]{:S(2)}) collective-permute-start(bf16[512,2048]{1,0:T(8,128)(2,1)} %rest_0_.1), channel_id=1, source_target_pairs={{0,1},{1,0},{2,3},{3,2},{4,5},{5,4},{6,7},{7,6},{8,9},{9,8},{10,11... | collective-permute-start | bytes 6291464 | tf_op jit(solution)/shard_map/ppermute | solution.py:363
  48.9 39.0 %collective-permute-start.4 = (bf16[512,2048]{1,0:T(8,128)(2,1)}, bf16[512,2048]{1,0:T(8,128)(2,1)}, u32[]{:S(2)}, u32[]{:S(2)}) collective-permute-start(bf16[512,2048]{1,0:T(8,128)(2,1)} %collective-permute-done.3.rest_2_), channel_id=1, source_target_pairs={{0,1},{1,0},{2,3},{3,2},{4,5},{5,4},{6,7},{7,6},{8,9},{9,8},{10,11... | collective-permute-start | bytes 6291464 | tf_op jit(solution)/shard_map/ppermute | solution.py:363
  48.9 4.9 %collective-permute-start = (s32[128,4]{0,1:T(4,128)S(1)}, s32[128,4]{0,1:T(4,128)S(1)}, u32[]{:S(2)}, u32[]{:S(2)}) collective-permute-start(s32[128,4]{0,1:T(4,128)S(1)} %bitcast.121), channel_id=1, source_target_pairs={{0,16},{16,0},{1,17},{17,1},{2,18},{18,2},{3,19},{19,3},{4,20},{20... | collective-permute-start | bytes 6152 | tf_op jit(solution)/shard_map/ppermute | solution.py:367
  51.8 4.5 %collective-permute-start.1 = (f32[128,4]{0,1:T(4,128)S(1)}, f32[128,4]{0,1:T(4,128)S(1)}, u32[]{:S(2)}, u32[]{:S(2)}) collective-permute-start(f32[128,4]{0,1:T(4,128)S(1)} %bitcast.126), channel_id=1, source_target_pairs={{0,16},{16,0},{1,17},{17,1},{2,18},{18,2},{3,19},{19,3},{4,20},{20... | collective-permute-start | bytes 6152 | tf_op jit(solution)/shard_map/ppermute | solution.py:368
  70.4 17.5 %all-to-all-start.1 = ((bf16[8,128,256]{2,1,0:T(8,128)(2,1)}), bf16[8,128,256]{2,1,0:T(8,128)(2,1)S(1)}, u32[]{:S(2)}, u32[]{:S(2)}) async-start(bf16[8,128,256]{2,1,0:T(8,128)(2,1)} %mixer.1), calls=%async_computation.1 | async-start | bytes 1048576 | tf_op jit(solution)/shard_map/all_to_all | solution.py:378
  88.0 1.6 copy-start
  96.7 43.1 %all-to-all-start.2 = ((bf16[16,32,2048]{2,1,0:T(8,128)(2,1)}), bf16[16,32,2048]{2,1,0:T(8,128)(2,1)}, u32[]{:S(2)}, u32[]{:S(2)}) async-start(bf16[16,32,2048]{2,1,0:T(8,128)(2,1)} %bitcast.111), calls=%async_computation.2 | async-start | bytes 4194304 | tf_op jit(solution)/shard_map/all_to_all | solution.py:395
  101.2 35.7 %collective-permute-start.5 = (bf16[128,2048]{1,0:T(8,128)(2,1)S(1)}, bf16[128,2048]{1,0:T(8,128)(2,1)S(1)}, u32[]{:S(2)}, u32[]{:S(2)}) collective-permute-start(bf16[128,2048]{1,0:T(8,128)(2,1)S(1)} %get-tuple-element.16), channel_id=1, source_target_pairs={{0,16},{16,0},{1,17},{17,1},{2,18},{18,2},{3,19},{19,3},{4,20},{20... | collective-permute-start | bytes 1572872 | tf_op jit(solution)/shard_map/ppermute | solution.py:403
  140.5 33.3 %copy-start.12 = (bf16[1,2048,1024]{2,1,0:T(8,128)(2,1)S(1)}, bf16[1,2048,1024]{2,1,0:T(8,128)(2,1)}, u32[]{:S(2)}) copy-start(bf16[1,2048,1024]{2,1,0:T(8,128)(2,1)} %param.34) | copy-start | bytes 12582916
  188.4 34.1 %all-to-all-start.4 = ((bf16[16,32,2048]{2,1,0:T(8,128)(2,1)}), bf16[16,32,2048]{2,1,0:T(8,128)(2,1)}, u32[]{:S(2)}, u32[]{:S(2)}) async-start(bf16[16,32,2048]{2,1,0:T(8,128)(2,1)} %bitcast.113), calls=%async_computation.4 | async-start | bytes 4194304 | tf_op jit(solution)/shard_map/all_to_all | solution.py:395
  225.0 43.1 %all-to-all-start.5 = ((bf16[16,32,2048]{2,1,0:T(8,128)(2,1)}), bf16[16,32,2048]{2,1,0:T(8,128)(2,1)}, u32[]{:S(2)}, u32[]{:S(2)}) async-start(bf16[16,32,2048]{2,1,0:T(8,128)(2,1)} %bitcast.114), calls=%async_computation.5 | async-start | bytes 4194304 | tf_op jit(solution)/shard_map/all_to_all | solution.py:395
  229.4 40.9 %collective-permute-start.6 = (bf16[128,2048]{1,0:T(8,128)(2,1)S(1)}, bf16[128,2048]{1,0:T(8,128)(2,1)S(1)}, u32[]{:S(2)}, u32[]{:S(2)}) collective-permute-start(bf16[128,2048]{1,0:T(8,128)(2,1)S(1)} %fusion.35), channel_id=1, source_target_pairs={{0,16},{16,0},{1,17},{17,1},{2,18},{18,2},{3,19},{19,3},{4,20},{20... | collective-permute-start | bytes 1572872 | tf_op jit(solution)/shard_map/ppermute | solution.py:414
  (1 other events, 1.4 us)

commit v3 on v2

--- a/solution.py
+++ b/solution.py
@@ -311,17 +311,54 @@
     return both[0] + both[1]
 
 
+def expert_body(rows_ref, gate_ref, up_ref, down_ref, o_ref, acc_ref):
+    j = pl.program_id(0)
+    rows = rows_ref[...]
+    gate_value = jnp.minimum(
+        jnp.dot(rows, gate_ref[...], preferred_element_type=f32), clamp_limit
+    )
+    up_value = jnp.clip(
+        jnp.dot(rows, up_ref[...], preferred_element_type=f32), -clamp_limit, clamp_limit
+    )
+    squash = 1.0 / (1.0 + jnp.exp(-sigmoid_slope * gate_value))
+    active = ((up_value + 1.0) * gate_value * squash).astype(bf16)
+    part = jnp.dot(active, down_ref[...], preferred_element_type=f32)
+    last = pl.num_programs(0) - 1
+
+    @pl.when(j == 0)
+    def _():
+        acc_ref[...] = part
+
+    @pl.when((j > 0) & (j < last))
+    def _():
+        acc_ref[...] += part
+
+    @pl.when(j == last)
+    def _():
+        o_ref[...] = (acc_ref[...] + part).astype(bf16)
+
+
 def expert_apply(rows, gate_mat, up_mat, down_mat):
-    gate_value = jnp.minimum(
-        jnp.dot(rows, gate_mat, preferred_element_type=jnp.float32), clamp_limit
-    )
-    up_value = jnp.clip(
-        jnp.dot(rows, up_mat, preferred_element_type=jnp.float32), -clamp_limit, clamp_limit
-    )
-    active = ((up_value + 1.0) * gate_value * jax.nn.sigmoid(sigmoid_slope * gate_value)).astype(
-        jnp.bfloat16
-    )
-    return jnp.dot(active, down_mat, preferred_element_type=jnp.float32).astype(jnp.bfloat16)
+    count, model = rows.shape
+    hidden = gate_mat.shape[1]
+    block = hidden // 4
+    wide = pl.BlockSpec((count, model), lambda j: (0, 0))
+    into = pl.BlockSpec((model, block), lambda j: (0, j))
+    return pl.pallas_call(
+        expert_body,
+        grid=(hidden // block,),
+        in_specs=[wide, into, into, pl.BlockSpec((block, model), lambda j: (j, 0))],
+        out_specs=wide,
+        out_shape=jax.ShapeDtypeStruct((count, model), bf16),
+        scratch_shapes=[pltpu.VMEM((count, model), f32)],
+        compiler_params=pltpu.CompilerParams(vmem_limit_bytes=48 * 1024 * 1024),
+        cost_estimate=pl.CostEstimate(
+            flops=6 * count * model * hidden,
+            bytes_accessed=2 * (3 * model * hidden + 2 * count * model),
+            transcendentals=count * hidden,
+        ),
+        name="expert",
+    )(rows, gate_mat, up_mat, down_mat)
 
 
 def per_device(
@@ -356,26 +393,33 @@
     capacity = 2 * token_count * top_count // experts_all
     swap = [(0, 1), (1, 0)]
 
+    def spread(pieces, bit):
+        steps_of = [(i, i ^ bit) for i in range(dp_count)]
+        fresh = {m ^ bit: lax.ppermute(piece, "dp", steps_of) for m, piece in pieces.items()}
+        return {**pieces, **fresh}
+
     pieces = {0: out_weight}
     bit = dp_count // 2
-    while bit:
-        steps_of = [(i, i ^ bit) for i in range(dp_count)]
-        fresh = {m ^ bit: lax.ppermute(piece, "dp", steps_of) for m, piece in pieces.items()}
-        pieces.update(fresh)
+    while bit > 1:
+        pieces = spread(pieces, bit)
         bit //= 2
-
-    other_routes = lax.ppermute(routing[0], "half", swap)
-    other_weight = lax.ppermute(route_weight[0], "half", swap)
 
     steps = step_raw[0].T.reshape(sp_count, -1, token_count)
     steps = jnp.pad(steps, ((0, 0), (0, STEP_ROWS - steps.shape[1]), (0, 0)))
     packed = pack_inputs(ssm_input[0], state_b[0], state_c[0], steps, sp_count)
     arrived_mix = lax.all_to_all(packed, sp_axes, split_axis=0, concat_axis=0, tiled=True)
-    arrived_mix, other_routes, other_weight = lax.optimization_barrier(
-        (arrived_mix, other_routes, other_weight)
-    )
     mixed_heads = mixer(arrived_mix, conv_x, conv_b, conv_c, decay_rate)
+    mixed_heads, pieces, routes, weights = lax.optimization_barrier(
+        (mixed_heads, pieces, routing[0], route_weight[0])
+    )
     mixed_tokens = lax.all_to_all(mixed_heads, sp_axes, split_axis=0, concat_axis=0, tiled=True)
+    other_routes = lax.ppermute(routes, "half", swap)
+    other_weight = lax.ppermute(weights, "half", swap)
+    if bit:
+        pieces = spread(pieces, bit)
+    mixed_tokens, other_routes, other_weight = lax.optimization_barrier(
+        (mixed_tokens, other_routes, other_weight)
+    )
 
     first = lax.axis_index("half") * group
     select, merge = slot_maps(routing[0], route_weight[0], first, group, capacity)

time: 272 us -> 269 us (0.989)
  matrix products: 39.8 us -> 7.08 us
  Pallas kernels: 24.6 us -> 47.9 us
  waiting for transfers between devices: 136 us -> 140 us
    all_to_all x1, waiting for transfers between devices: 0.01 us -> 36.6 us  [per_device(): lax.all_to_all(packed, sp_axes, split_axis=0, concat_axis=0, tiled=True)]
    dot_general x4 -> x0, matrix products: 32.2 us -> none  [the longest x2 22 us: expert_apply(): jnp.dot(active, down_mat, preferred_element_type=jnp.float32)]
    ppermute x5, waiting for transfers between devices: 37.3 us -> 11.8 us  [the longest x1 11.8 us: per_device(): other_routes = lax.ppermute(routes, 'half', swap)]
    pallas_call x0 -> x2, Pallas kernels: none -> 22.9 us  [expert_apply(): pl.pallas_call(expert_body, grid=(hidden // block,), in_specs=[wide, into...]
    all_to_all x1, waiting for transfers between devices: 13.1 us -> 0.01 us  [per_device(): lax.all_to_all(mixed_heads, sp_axes, split_axis=0, concat_axis=0, tiled=T...]
    all_to_all x3, waiting for transfers between devices: 51.2 us -> 55.3 us  [exchange(): lax.all_to_all(slots.reshape(group, capacity, model_width), group_axes, s...]
  transfers between devices with their start and end apart: 12 -> 12, of which waited for: 8 -> 6; matrix products, arithmetic and copies ran while one was open for 8% -> 1% of each run, Pallas kernels for 7% -> 10%
where the time goes in v3:
time: 269 us; the launch traced here: 268 us
  waiting for transfers between devices  140 us (52%)
  Pallas kernels  47.9 us (18%)
  blocking collectives  32.3 us (12%)
  starting transfers between devices  31.2 us (12%)
  matrix products  7.08 us (3%)
  local copies, waits for them, and re-layouts  5.84 us (2%)
  other arithmetic  3.5 us (1%)
    all_to_all x3, waiting for transfers between devices, exchange(): lax.all_to_all(slots.reshape(group, capacity, model_width), group_axes, s...  55.3 us
    all_to_all x1, waiting for transfers between devices, per_device(): lax.all_to_all(packed, sp_axes, split_axis=0, concat_axis=0, tiled=True)  36.6 us
    ppermute x1, waiting for transfers between devices, per_device(): other_rows = lax.ppermute(rows, 'half', swap)  36.2 us
    all_to_all x1, blocking collectives, exchange(): lax.all_to_all(slots.reshape(group, capacity, model_width), group_axes, s...  32.3 us
    pallas_call x2, Pallas kernels, expert_apply(): pl.pallas_call(expert_body, grid=(hidden // block,), in_specs=[wide, into...  22.9 us
    pallas_call x1, Pallas kernels, mixer(): pl.pallas_call(mixer_body, out_shape=jax.ShapeDtypeStruct((blocks, tokens...  14.1 us
    all_to_all x3, starting transfers between devices, exchange(): lax.all_to_all(slots.reshape(group, capacity, model_width), group_axes, s...  12 us
    ppermute x1, waiting for transfers between devices, per_device(): other_routes = lax.ppermute(routes, 'half', swap)  11.8 us
  transfers between devices with their start and end apart: 12, of which 6 were waited for; matrix products, arithmetic and copies ran while one was open for 1% of the time, Pallas kernels for 10%

profile of v3, /device:TPU:0, one launch (start us, length us, event | category | flops | bytes accessed | tf_op | source)
XLA Modules:
  0.0 268.0 jit_solution(551525919695177513)
XLA Ops:
  1.3 5.4 %pack_inputs.1 = bf16[8,400,256]{2,1,0:T(8,128)(2,1)} custom-call(bf16[128,2048]{1,0:T(8,128)(2,1)} %bitcast.88, bf16[128,2048]{1,0:T(8,128)(2,1)} %bitcast.89, bf16[128,2048]{1,0:T(8,128)(2,1)} %bitcast.90, bf16[8,16,128]{2,1,0:T(8,128)(2,1)} %pad.8.s_ref), custom_call_target="tpu_custom_call" | custom-call | tf_op jit(solution)/shard_map/pack_inputs/pallas_call | solution.py:35
  6.7 7.4 %all-to-all-start = ((bf16[8,400,256]{2,1,0:T(8,128)(2,1)}), bf16[8,400,256]{2,1,0:T(8,128)(2,1)S(1)}, u32[]{:S(2)}, u32[]{:S(2)}) async-start(bf16[8,400,256]{2,1,0:T(8,128)(2,1)} %pack_inputs.1), calls=%async_computation | async-start | bytes 3276800 | tf_op jit(solution)/shard_map/all_to_all | solution.py:410
  14.2 1.6 collective-permute-start
  16.0 36.6 %all-to-all-done.in_ref = bf16[8,400,256]{2,1,0:T(8,128)(2,1)S(1)} async-done(((bf16[8,400,256]{2,1,0:T(8,128)(2,1)}), bf16[8,400,256]{2,1,0:T(8,128)(2,1)S(1)}, u32[]{:S(2)}, u32[]{:S(2)}) %all-to-all-start) | async-done | bytes 1638432 | tf_op jit(solution)/shard_map/all_to_all | solution.py:410
  52.6 14.1 %mixer.1 = bf16[8,128,256]{2,1,0:T(8,128)(2,1)} custom-call(bf16[8,400,256]{2,1,0:T(8,128)(2,1)S(1)} %all-to-all-done.in_ref, f32[7,256]{1,0:T(8,128)S(1)} %copy-done.4, f32[7,256]{1,0:T(8,128)S(1)} %copy-done.5, f32[7,256]{1,0:T(8,128)S(1)} %copy-done.6, f32[16,1]{1,0:T(8,128)S(1)} %pad.9.rate_ref), custom_call_target="tpu_custom_call" | custom-call | tf_op jit(solution)/shard_map/mixer/pallas_call | solution.py:201
  67.2 3.6 %all-to-all-start.1 = ((bf16[8,128,256]{2,1,0:T(8,128)(2,1)}), bf16[8,128,256]{2,1,0:T(8,128)(2,1)S(1)}, u32[]{:S(2)}, u32[]{:S(2)}) async-start(bf16[8,128,256]{2,1,0:T(8,128)(2,1)} %mixer.1), calls=%async_computation.1 | async-start | bytes 1048576 | tf_op jit(solution)/shard_map/all_to_all | solution.py:415
  70.9 2.9 %collective-permute-start.1 = (s32[128,4]{0,1:T(4,128)S(1)}, s32[128,4]{0,1:T(4,128)S(1)}, u32[]{:S(2)}, u32[]{:S(2)}) collective-permute-start(s32[128,4]{0,1:T(4,128)S(1)} %bitcast.92), channel_id=1, source_target_pairs={{0,16},{16,0},{1,17},{17,1},{2,18},{18,2},{3,19},{19,3},{4,20},{20... | collective-permute-start | bytes 6152 | tf_op jit(solution)/shard_map/ppermute | solution.py:416
  74.0 11.8 %collective-permute-done.1 = s32[128,4]{0,1:T(4,128)S(1)} collective-permute-done((s32[128,4]{0,1:T(4,128)S(1)}, s32[128,4]{0,1:T(4,128)S(1)}, u32[]{:S(2)}, u32[]{:S(2)}) %collective-permute-start.1) | collective-permute-done | bytes 2080 | tf_op jit(solution)/shard_map/ppermute | solution.py:416
  88.4 5.5 %project.1 = (f32[128,2048]{1,0:T(8,128)S(1)}, bf16[128,2048]{1,0:T(8,128)(2,1)S(1)}) custom-call(s32[1]{0:T(128)} %bitcast.place_ref, bf16[8,128,256]{2,1,0:T(8,128)(2,1)S(1)} %all-to-all-done.1.mix_ref, bf16[128,2048]{1,0:T(8,128)(2,1)S(1)} %bitcast.82, f32[1,2048]{1,0:T(1,128)S(1)} %bitcast.84, bf16[128,2048]{1,0:T(8,128)(2,1)S(1)} %bitcast.83, ...), custom_call_target="tpu_custom_call" | custom-call | tf_op jit(solution)/shard_map/project/pallas_call | solution.py:265
  94.7 2.0 convolution_convert_fusion.1
  96.7 3.8 %all-to-all-start.2 = ((bf16[16,32,2048]{2,1,0:T(8,128)(2,1)}), bf16[16,32,2048]{2,1,0:T(8,128)(2,1)S(1)}, u32[]{:S(2)}, u32[]{:S(2)}) async-start(bf16[16,32,2048]{2,1,0:T(8,128)(2,1)} %bitcast.86), calls=%async_computation.2 | async-start | bytes 4194304 | tf_op jit(solution)/shard_map/all_to_all | solution.py:439
  100.5 1.5 collective-permute-start.5
  102.0 36.2 %collective-permute-done.5 = bf16[128,2048]{1,0:T(8,128)(2,1)} collective-permute-done((bf16[128,2048]{1,0:T(8,128)(2,1)}, bf16[128,2048]{1,0:T(8,128)(2,1)}, u32[]{:S(2)}, u32[]{:S(2)}) %collective-permute-start.5) | collective-permute-done | bytes 524320 | tf_op jit(solution)/shard_map/ppermute | solution.py:447
  139.2 1.7 convolution_convert_fusion
  140.9 32.3 %all_to_all.30 = bf16[16,32,2048]{2,1,0:T(8,128)(2,1)S(1)} all-to-all(bf16[16,32,2048]{2,1,0:T(8,128)(2,1)S(1)} %bitcast.87), channel_id=1, replica_groups=mesh['half'=2,'rest'=4,'dp'=4] {'rest','dp'}, dimensions={0} | all-to-all | bytes 4194304 | tf_op jit(solution)/shard_map/all_to_all | solution.py:439
  173.3 10.8 %expert.3 = bf16[512,2048]{1,0:T(8,128)(2,1)S(1)} custom-call(bf16[512,2048]{1,0:T(8,128)(2,1)S(1)} %bitcast.81, bf16[2048,1024]{1,0:T(8,128)(2,1)} %bitcast.101, bf16[2048,1024]{1,0:T(8,128)(2,1)} %bitcast.103, bf16[1024,2048]{1,0:T(8,128)(2,1)} %bitcast.105), custom_call_target="tpu_custom_call" | custom-call | flops 6442450944 | bytes 16777216 | tf_op jit(solution)/shard_map/expert/pallas_call | solution.py:347
  185.4 4.4 %all-to-all-start.4 = ((bf16[16,32,2048]{2,1,0:T(8,128)(2,1)}), bf16[16,32,2048]{2,1,0:T(8,128)(2,1)}, u32[]{:S(2)}, u32[]{:S(2)}) async-start(bf16[16,32,2048]{2,1,0:T(8,128)(2,1)} %bitcast.80), calls=%async_computation.4 | async-start | bytes 4194304 | tf_op jit(solution)/shard_map/all_to_all | solution.py:439
  190.0 12.1 %expert.2 = bf16[512,2048]{1,0:T(8,128)(2,1)} custom-call(bf16[512,2048]{1,0:T(8,128)(2,1)S(1)} %bitcast.79, bf16[2048,1024]{1,0:T(8,128)(2,1)} %bitcast.102, bf16[2048,1024]{1,0:T(8,128)(2,1)} %bitcast.104, bf16[1024,2048]{1,0:T(8,128)(2,1)} %bitcast.106), custom_call_target="tpu_custom_call" | custom-call | flops 6442450944 | bytes 16777216 | tf_op jit(solution)/shard_map/expert/pallas_call | solution.py:347
  202.1 17.4 %all-to-all-done.4 = bf16[16,32,2048]{2,1,0:T(8,128)(2,1)} async-done(((bf16[16,32,2048]{2,1,0:T(8,128)(2,1)}), bf16[16,32,2048]{2,1,0:T(8,128)(2,1)}, u32[]{:S(2)}, u32[]{:S(2)}) %all-to-all-start.4) | async-done | bytes 2097184 | tf_op jit(solution)/shard_map/all_to_all | solution.py:439
  219.5 2.3 convolution_bitcast_fusion.1
  222.7 3.7 %all-to-all-start.5 = ((bf16[16,32,2048]{2,1,0:T(8,128)(2,1)}), bf16[16,32,2048]{2,1,0:T(8,128)(2,1)S(1)}, u32[]{:S(2)}, u32[]{:S(2)}) async-start(bf16[16,32,2048]{2,1,0:T(8,128)(2,1)} %bitcast.34), calls=%async_computation.5 | async-start | bytes 4194304 | tf_op jit(solution)/shard_map/all_to_all | solution.py:439
  226.5 1.6 collective-permute-start.6
  228.1 36.9 %all-to-all-done.5 = bf16[16,32,2048]{2,1,0:T(8,128)(2,1)S(1)} async-done(((bf16[16,32,2048]{2,1,0:T(8,128)(2,1)}), bf16[16,32,2048]{2,1,0:T(8,128)(2,1)S(1)}, u32[]{:S(2)}, u32[]{:S(2)}) %all-to-all-start.5) | async-done | bytes 2097184 | tf_op jit(solution)/shard_map/all_to_all | solution.py:439
  265.8 2.2 fusion.10
  (53 shorter events, 9.8 us)
Async XLA Ops:
  6.7 9.1 %copy-start.11 = (f32[2,4]{1,0:T(2,128)S(1)}, f32[2,4]{1,0:T(2,128)}, u32[]{:S(2)}) copy-start(f32[2,4]{1,0:T(2,128)} %param.27) | copy-start | bytes 100
  6.7 45.9 %copy-start.4 = (f32[7,256]{1,0:T(8,128)S(1)}, f32[7,256]{1,0:T(8,128)}, u32[]{:S(2)}) copy-start(f32[7,256]{1,0:T(8,128)} %tx_ref.1) | copy-start | bytes 21508
  6.7 45.9 %copy-start.5 = (f32[7,256]{1,0:T(8,128)S(1)}, f32[7,256]{1,0:T(8,128)}, u32[]{:S(2)}) copy-start(f32[7,256]{1,0:T(8,128)} %tb_ref.1) | copy-start | bytes 21508
  6.7 45.9 %copy-start.6 = (f32[7,256]{1,0:T(8,128)S(1)}, f32[7,256]{1,0:T(8,128)}, u32[]{:S(2)}) copy-start(f32[7,256]{1,0:T(8,128)} %tc_ref.1) | copy-start | bytes 21508
  6.7 45.8 %all-to-all-start = ((bf16[8,400,256]{2,1,0:T(8,128)(2,1)}), bf16[8,400,256]{2,1,0:T(8,128)(2,1)S(1)}, u32[]{:S(2)}, u32[]{:S(2)}) async-start(bf16[8,400,256]{2,1,0:T(8,128)(2,1)} %pack_inputs.1), calls=%async_computation | async-start | bytes 3276800 | tf_op jit(solution)/shard_map/all_to_all | solution.py:410
  14.2 56.7 %copy-start.9 = (s32[1,128,4]{1,2,0:T(4,128)S(1)}, s32[1,128,4]{1,2,0:T(4,128)}, u32[]{:S(2)}) copy-start(s32[1,128,4]{1,2,0:T(4,128)} %param.31) | copy-start | bytes 6148
  14.2 59.6 %copy-start.10 = (f32[1,128,4]{1,2,0:T(4,128)S(1)}, f32[1,128,4]{1,2,0:T(4,128)}, u32[]{:S(2)}) copy-start(f32[1,128,4]{1,2,0:T(4,128)} %param.32) | copy-start | bytes 6148
  14.2 72.1 %copy-start.7 = (f32[2048]{0:T(1024)S(1)}, f32[2048]{0:T(1024)}, u32[]{:S(2)}) copy-start(f32[2048]{0:T(1024)} %param.28) | copy-start | bytes 24580
  14.2 72.1 %copy-start.8 = (f32[2048]{0:T(1024)S(1)}, f32[2048]{0:T(1024)}, u32[]{:S(2)}) copy-start(f32[2048]{0:T(1024)} %param.30) | copy-start | bytes 24580
  14.2 52.5 %collective-permute-start = (bf16[512,2048]{1,0:T(8,128)(2,1)}, bf16[512,2048]{1,0:T(8,128)(2,1)}, u32[]{:S(2)}, u32[]{:S(2)}) collective-permute-start(bf16[512,2048]{1,0:T(8,128)(2,1)} %rest_0_), channel_id=1, source_target_pairs={{0,2},{1,3},{2,0},{3,1},{4,6},{5,7},{6,4},{7,5},{8,10},{9,11},{10,... | collective-permute-start | bytes 6291464 | tf_op jit(solution)/shard_map/ppermute | solution.py:398
  66.7 19.6 %collective-permute-start.3 = (bf16[512,2048]{1,0:T(8,128)(2,1)}, bf16[512,2048]{1,0:T(8,128)(2,1)}, u32[]{:S(2)}, u32[]{:S(2)}) collective-permute-start(bf16[512,2048]{1,0:T(8,128)(2,1)} %rest_0_), channel_id=1, source_target_pairs={{0,1},{1,0},{2,3},{3,2},{4,5},{5,4},{6,7},{7,6},{8,9},{9,8},{10,11... | collective-permute-start | bytes 6291464 | tf_op jit(solution)/shard_map/ppermute | solution.py:398
  66.7 19.6 %collective-permute-start.4 = (bf16[512,2048]{1,0:T(8,128)(2,1)}, bf16[512,2048]{1,0:T(8,128)(2,1)}, u32[]{:S(2)}, u32[]{:S(2)}) collective-permute-start(bf16[512,2048]{1,0:T(8,128)(2,1)} %collective-permute-done.rest_2_), channel_id=1, source_target_pairs={{0,1},{1,0},{2,3},{3,2},{4,5},{5,4},{6,7},{7,6},{8,9},{9,8},{10,11... | collective-permute-start | bytes 6291464 | tf_op jit(solution)/shard_map/ppermute | solution.py:398
  67.2 18.5 %all-to-all-start.1 = ((bf16[8,128,256]{2,1,0:T(8,128)(2,1)}), bf16[8,128,256]{2,1,0:T(8,128)(2,1)S(1)}, u32[]{:S(2)}, u32[]{:S(2)}) async-start(bf16[8,128,256]{2,1,0:T(8,128)(2,1)} %mixer.1), calls=%async_computation.1 | async-start | bytes 1048576 | tf_op jit(solution)/shard_map/all_to_all | solution.py:415
  70.9 14.9 %collective-permute-start.1 = (s32[128,4]{0,1:T(4,128)S(1)}, s32[128,4]{0,1:T(4,128)S(1)}, u32[]{:S(2)}, u32[]{:S(2)}) collective-permute-start(s32[128,4]{0,1:T(4,128)S(1)} %bitcast.92), channel_id=1, source_target_pairs={{0,16},{16,0},{1,17},{17,1},{2,18},{18,2},{3,19},{19,3},{4,20},{20... | collective-permute-start | bytes 6152 | tf_op jit(solution)/shard_map/ppermute | solution.py:416
  73.8 12.0 %collective-permute-start.2 = (f32[128,4]{0,1:T(4,128)S(1)}, f32[128,4]{0,1:T(4,128)S(1)}, u32[]{:S(2)}, u32[]{:S(2)}) collective-permute-start(f32[128,4]{0,1:T(4,128)S(1)} %bitcast.97), channel_id=1, source_target_pairs={{0,16},{16,0},{1,17},{17,1},{2,18},{18,2},{3,19},{19,3},{4,20},{20... | collective-permute-start | bytes 6152 | tf_op jit(solution)/shard_map/ppermute | solution.py:417
  86.3 1.0 copy-start.1
  87.4 1.0 copy-start.2
  93.9 0.8 copy-start.3
  96.7 42.5 %all-to-all-start.2 = ((bf16[16,32,2048]{2,1,0:T(8,128)(2,1)}), bf16[16,32,2048]{2,1,0:T(8,128)(2,1)S(1)}, u32[]{:S(2)}, u32[]{:S(2)}) async-start(bf16[16,32,2048]{2,1,0:T(8,128)(2,1)} %bitcast.86), calls=%async_computation.2 | async-start | bytes 4194304 | tf_op jit(solution)/shard_map/all_to_all | solution.py:439
  100.5 37.7 %collective-permute-start.5 = (bf16[128,2048]{1,0:T(8,128)(2,1)}, bf16[128,2048]{1,0:T(8,128)(2,1)}, u32[]{:S(2)}, u32[]{:S(2)}) collective-permute-start(bf16[128,2048]{1,0:T(8,128)(2,1)} %copy-done.3), channel_id=1, source_target_pairs={{0,16},{16,0},{1,17},{17,1},{2,18},{18,2},{3,19},{19,3},{4,20},{20... | collective-permute-start | bytes 1572872 | tf_op jit(solution)/shard_map/ppermute | solution.py:447
  184.0 1.3 copy-start
  185.4 34.1 %all-to-all-start.4 = ((bf16[16,32,2048]{2,1,0:T(8,128)(2,1)}), bf16[16,32,2048]{2,1,0:T(8,128)(2,1)}, u32[]{:S(2)}, u32[]{:S(2)}) async-start(bf16[16,32,2048]{2,1,0:T(8,128)(2,1)} %bitcast.80), calls=%async_computation.4 | async-start | bytes 4194304 | tf_op jit(solution)/shard_map/all_to_all | solution.py:439
  222.7 42.3 %all-to-all-start.5 = ((bf16[16,32,2048]{2,1,0:T(8,128)(2,1)}), bf16[16,32,2048]{2,1,0:T(8,128)(2,1)S(1)}, u32[]{:S(2)}, u32[]{:S(2)}) async-start(bf16[16,32,2048]{2,1,0:T(8,128)(2,1)} %bitcast.34), calls=%async_computation.5 | async-start | bytes 4194304 | tf_op jit(solution)/shard_map/all_to_all | solution.py:439
  226.5 39.4 %collective-permute-start.6 = (bf16[128,2048]{1,0:T(8,128)(2,1)}, bf16[128,2048]{1,0:T(8,128)(2,1)}, u32[]{:S(2)}, u32[]{:S(2)}) collective-permute-start(bf16[128,2048]{1,0:T(8,128)(2,1)} %fusion.9), channel_id=1, source_target_pairs={{0,16},{16,0},{1,17},{17,1},{2,18},{18,2},{3,19},{19,3},{4,20},{20... | collective-permute-start | bytes 1572872 | tf_op jit(solution)/shard_map/ppermute | solution.py:458
